TPU v7x, 256 devices: a whole 4x4x8 slice. The times are simulated.
256 devices in a mesh: kv: 64 (over z, y, core), tp: 4 (over x).
Axes of the slice: x: 4, y: 4, z: 8, core: 2. Of those that a mesh axis runs over, the one named last changes fastest.
Arguments:
- tokens: bfloat16 [49152, 2048], P('kv'), may hold values from -6 to 6
- w_query: bfloat16 [2048, 4096], P(None, 'tp'), may hold values from -3.1819805 to 3.1819805
- w_latent: bfloat16 [2048, 256], replicated, may hold values from -0.13258252 to 0.13258252
- latent_gain: float32 [256], replicated, may hold values from 0.1 to 1.9
- w_output: bfloat16 [4096, 2048], P('tp'), may hold values from -2 to 2
- chosen: int32 [768, 32], P('kv'), may hold values from -1 to 767, as said below
Outputs:
- attended: bfloat16 [49152, 2048], P(('kv', 'tp'))
- log_total: float32 [49152, 16], P('kv', 'tp')
Inputs may be any that keep to these rules, and one draw needn't show every extreme that they name: `chosen`: row g names blocks at or before block g, no block twice; entry 0 is g itself; entries -1 name nothing and stand after the others. The 12 rows of one device together name exactly 2 distinct blocks of every earlier device's positions and none of a later device's.
All inputs are finite; a program needn't handle non-finite values.
Results may differ from a plain program's by a relative error of at most 0.01.
Values may be sent and summed in bfloat16 or wider, within the bound.
A program may use at most 192 MiB of HBM per device.

v0:
```python
import math

import jax
import jax.numpy as jnp
from jax import lax
from jax.sharding import PartitionSpec as P

CAP = 2


epsilon = 1e-06


def split_up(value, dim, devices):
    lengths = value.shape
    blocks = value.reshape(*lengths[:dim], devices, lengths[dim] // devices, *lengths[dim + 1 :])
    return jnp.moveaxis(blocks, dim, 0)


def summed_on_arrival(value, axis, dim):
    devices = lax.axis_size(axis)
    blocks = lax.all_to_all(split_up(value, dim, devices), axis, 0, 0, tiled=True)
    return jnp.sum(blocks.astype(jnp.float32), axis=0)


def latents_of(tokens, w_latent, latent_gain):
    projected = jnp.dot(tokens, w_latent, preferred_element_type=jnp.float32)
    inv_rms = lax.rsqrt(jnp.mean(projected * projected, axis=-1, keepdims=True) + epsilon)
    return (projected * inv_rms * latent_gain).astype(jnp.bfloat16)


def attend(query_part, key_rows, picked, query_blocks, blk_len, score_scale):
    group_size, picks_each = picked.shape
    offsets = jnp.arange(blk_len, dtype=jnp.int32)
    key_pos = (picked[:, :, None] * blk_len + offsets[None, None, :]).reshape(
        group_size, picks_each * blk_len
    )
    usable = jnp.repeat(picked >= 0, blk_len, axis=1)
    query_pos = query_blocks[:, None] * blk_len + offsets[None, :]
    allowed = usable[:, None, :] & (key_pos[:, None, :] <= query_pos[:, :, None])
    scores = (
        jnp.einsum("gqhr,gkr->ghqk", query_part, key_rows, preferred_element_type=jnp.float32)
        * score_scale
    )
    scores = jnp.where(allowed[:, None, :, :], scores, -jnp.inf)
    peak_score = jnp.max(scores, axis=3, keepdims=True)
    raised = jnp.exp(scores - peak_score)
    total_mass = jnp.sum(raised, axis=3)
    weights = raised.astype(jnp.bfloat16)
    summed = jnp.einsum("ghqk,gkr->gqhr", weights, key_rows, preferred_element_type=jnp.float32)
    mass_t = jnp.transpose(total_mass, (0, 2, 1))
    heads_out = (summed / mass_t[..., None]).astype(jnp.bfloat16)
    log_part = jnp.transpose(peak_score[..., 0], (0, 2, 1)) + jnp.log(mass_t)
    return (heads_out, log_part)


def slot_table(hit_mask):
    counted = jnp.cumsum(hit_mask.astype(jnp.int32), axis=1) - 1
    slot_ids = jnp.arange(CAP, dtype=jnp.int32)
    match_mask = hit_mask[:, None, :] & (counted[:, None, :] == slot_ids[None, :, None])
    places = jnp.arange(hit_mask.shape[1], dtype=jnp.int32)
    found = jnp.sum(jnp.where(match_mask, places[None, None, :], 0), axis=2)
    slot_list = jnp.where(jnp.any(match_mask, axis=2), found, -1)
    return (counted, slot_list)


def local(tokens, w_query, w_latent, latent_gain, w_output, chosen):
    tok_rows = tokens.shape[0]
    lat_rank = w_latent.shape[1]
    head_count = w_query.shape[1] // lat_rank
    per_device, picks_each = chosen.shape
    blk_len = tok_rows // per_device
    devices = lax.axis_size("kv")
    my_index = lax.axis_index("kv")
    latent = latents_of(tokens, w_latent, latent_gain)
    safe_ids = jnp.maximum(chosen, 0)
    own_blocks = latent.reshape(per_device, blk_len, lat_rank)
    flat_ids = chosen.reshape(per_device * picks_each)
    every_block = jnp.arange(devices * per_device, dtype=jnp.int32)
    owners = jnp.arange(devices, dtype=jnp.int32)
    others = (owners != my_index)[:, None]
    wanted = (
        jnp.any(flat_ids[:, None] == every_block[None, :], axis=0).reshape(devices, per_device)
        & others
    )
    counted, request = slot_table(wanted)
    reply_blocks = jnp.take(
        own_blocks,
        jnp.maximum(lax.all_to_all(request, "kv", split_axis=0, concat_axis=0, tiled=True), 0),
        axis=0,
    )
    fetched = lax.all_to_all(reply_blocks, "kv", split_axis=0, concat_axis=0, tiled=True)
    key_table = jnp.concatenate(
        [own_blocks, fetched.reshape(devices * CAP, blk_len, lat_rank)], axis=0
    )
    owner_of = safe_ids // per_device
    rank_of = jnp.take(counted.reshape(devices * per_device), safe_ids)
    lookup = jnp.where(
        owner_of == my_index,
        safe_ids - my_index * per_device,
        per_device + owner_of * CAP + rank_of,
    )
    queries = jnp.dot(tokens, w_query, preferred_element_type=jnp.float32).astype(jnp.bfloat16)
    queries = queries.reshape(per_device, blk_len, head_count, lat_rank)
    group_size = math.gcd(per_device, max(1, 512 // (blk_len * head_count)))
    first_block = my_index * per_device
    score_scale = lat_rank ** (-0.5)

    def one_group(offset):
        picked = lax.dynamic_slice_in_dim(chosen, offset, group_size, 0)
        located = lax.dynamic_slice_in_dim(lookup, offset, group_size, 0)
        query_part = lax.dynamic_slice_in_dim(queries, offset, group_size, 0)
        key_rows = jnp.take(key_table, located, axis=0).reshape(
            group_size, picks_each * blk_len, lat_rank
        )
        query_blocks = first_block + offset + jnp.arange(group_size, dtype=jnp.int32)
        return attend(query_part, key_rows, picked, query_blocks, blk_len, score_scale)

    group_starts = jnp.arange(0, per_device, group_size, dtype=jnp.int32)
    heads_out, log_total = lax.map(one_group, group_starts)
    heads_flat = heads_out.reshape(tok_rows, head_count * lat_rank)
    log_total = log_total.reshape(tok_rows, head_count)
    attended = summed_on_arrival(
        jnp.dot(heads_flat, w_output, preferred_element_type=jnp.float32).astype(jnp.bfloat16),
        "tp",
        0,
    ).astype(jnp.bfloat16)
    return (attended, log_total)


def solution(mesh):
    placed = (P("kv", None), P(None, "tp"), P(), P(), P("tp", None), P("kv", None))
    return jax.shard_map(
        local,
        mesh=mesh,
        in_specs=placed,
        out_specs=(P(("kv", "tp"), None), P("kv", "tp")),
        check_vma=False,
    )
```

profile of v0, /device:TPU:48, one launch (start us, length us, event | category | flops | bytes accessed | tf_op | source)
XLA Modules:
  0.0 311.8 jit_solution(11105900945250541219)
XLA Ops:
  0.7 0.9 eq.36
  3.2 11.7 %all-to-all-start = ((s32[64,1,2]{2,1,0:T(1,128)}), s32[64,1,2]{2,1,0:T(1,128)}, u32[]{:S(2)}, u32[]{:S(2)}) async-start(s32[64,1,2]{2,1,0:T(1,128)} %copy.26), calls=%async_computation | async-start | bytes 65536 | tf_op jit(solution)/shard_map/all_to_all | solution.py:89
  14.9 2.3 multiply_reduce_fusion
  17.4 4.3 %all-to-all-done = s32[64,1,2]{2,1,0:T(1,128)} async-done(((s32[64,1,2]{2,1,0:T(1,128)}), s32[64,1,2]{2,1,0:T(1,128)}, u32[]{:S(2)}, u32[]{:S(2)}) %all-to-all-start) | async-done | bytes 544 | tf_op jit(solution)/shard_map/all_to_all | solution.py:89
  21.8 1.5 maximum_reduce_fusion
  23.2 0.9 reshape.186
  24.1 1.4 maximum_compare_fusion
  25.5 0.8 copy.27
  26.5 2.8 gather_fusion.2
  29.3 4.6 %broadcast_select_fusion = bf16[64,2,64,256]{3,2,1,0:T(8,128)(2,1)} fusion(bf16[64,2,64,256]{3,2,1,0:T(8,128)(2,1)} %bitcast.82, pred[64,2]{1,0:T(8,128)(4,1)S(1)} %copy.28), kind=kLoop, calls=%fused_computation.34 | loop fusion | flops 2097152 | bytes 8388736 | tf_op jit(solution)/shard_map/jit(_take)/select_n | solution.py:87
  33.9 8.3 %all-to-all-start.1 = ((bf16[64,2,64,256]{3,2,1,0:T(8,128)(2,1)}), bf16[64,2,64,256]{3,2,1,0:T(8,128)(2,1)}, u32[]{:S(2)}, u32[]{:S(2)}) async-start(bf16[64,2,64,256]{3,2,1,0:T(8,128)(2,1)} %broadcast_select_fusion), calls=%async_computation.1 | async-start | bytes 8388608 | tf_op jit(solution)/shard_map/all_to_all | solution.py:92
  42.2 0.9 sub.30
  43.7 0.8 reshape.178
  45.0 2.0 gather_fusion.1
  47.7 6.7 %convolution_convert_fusion.1 = bf16[768,1024]{1,0:T(8,128)(2,1)} fusion(bf16[768,2048]{1,0:T(8,128)(2,1)S(1)} %copy-done, bf16[2048,1024]{1,0:T(8,128)(2,1)} %param.9), kind=kOutput, calls=%fused_computation.36 | convolution fusion | flops 3222011904 | bytes 8912896 | tf_op jit(solution)/shard_map/dot_general | solution.py:103
  54.5 3.9 %reshape.164 = bf16[12,64,4,256]{3,2,1,0:T(4,128)(2,1)} reshape(bf16[768,1024]{1,0:T(8,128)(2,1)} %convolution_convert_fusion.1) | data formatting | bytes 3145728 | tf_op jit(solution)/shard_map/reshape | solution.py:104
  58.3 1.3 add_select_fusion.1
  59.6 77.8 %all-to-all-done.1 = bf16[64,2,64,256]{3,2,1,0:T(8,128)(2,1)} async-done(((bf16[64,2,64,256]{3,2,1,0:T(8,128)(2,1)}), bf16[64,2,64,256]{3,2,1,0:T(8,128)(2,1)}, u32[]{:S(2)}, u32[]{:S(2)}) %all-to-all-start.1) | async-done | bytes 4194336 | tf_op jit(solution)/shard_map/all_to_all | solution.py:92
  137.5 4.6 %pad_maximum_fusion = bf16[140,64,256]{2,1,0:T(8,128)(2,1)} fusion(bf16[128,64,256]{2,1,0:T(8,128)(2,1)} %bitcast.15, bf16[12,64,256]{2,1,0:T(8,128)(2,1)S(1)} %bitcast.81), kind=kLoop, calls=%fused_computation.33 | loop fusion | flops 2293760 | bytes 9175040 | tf_op jit(solution)/shard_map/concatenate | solution.py:93
  142.1 114.5 %while.12 = (s32[]{:T(128)}, bf16[6,2,64,4,256]{4,3,2,1,0:T(4,128)(2,1)}, f32[6,2,64,4]{2,1,0,3:T(2,128)}, s32[6]{0:T(128)S(1)}, s32[12,32]{1,0:T(8,128)}, /*ind...) while((s32[]{:T(128)}, ...), condition=%wide.region_8.9_spmd, body=%wide.region_5.8_spmd.sunk | while | flops 1082922112 | bytes 35847144 | solution.py:120
  144.6 0.7 compare_and_fusion.5
  145.4 4.4 %gather_fusion = bf16[64,64,256]{2,1,0:T(8,128)(2,1)} fusion(bf16[140,64,256]{2,1,0:T(8,128)(2,1)} %get-tuple-element.209, s32[1024]{0:T(1024)S(1)} %pad_clamp_fusion.4), kind=kCustom, calls=%fused_computation.clone.1 | custom fusion | bytes 4194560 | tf_op jit(solution)/shard_map/while/body/eval_jaxpr/jit(_take)/gather | solution.py:113
  149.9 2.9 bitcast_select_fusion.3
  154.3 1.0 constant_dynamic-slice_fusion.4
  155.3 2.6 fusion.52
  159.5 0.8 fusion.54
  160.3 0.9 copy_dynamic-update-slice_fusion.4
  163.7 0.7 compare_and_fusion.5
  164.5 4.4 %gather_fusion = bf16[64,64,256]{2,1,0:T(8,128)(2,1)} fusion(bf16[140,64,256]{2,1,0:T(8,128)(2,1)} %get-tuple-element.209, s32[1024]{0:T(1024)S(1)} %pad_clamp_fusion.4), kind=kCustom, calls=%fused_computation.clone.1 | custom fusion | bytes 4194560 | tf_op jit(solution)/shard_map/while/body/eval_jaxpr/jit(_take)/gather | solution.py:113
  169.0 2.9 bitcast_select_fusion.3
  173.4 1.0 constant_dynamic-slice_fusion.4
  174.4 2.6 fusion.52
  178.6 0.8 fusion.54
  179.4 0.9 copy_dynamic-update-slice_fusion.4
  182.8 0.7 compare_and_fusion.5
  183.6 4.4 %gather_fusion = bf16[64,64,256]{2,1,0:T(8,128)(2,1)} fusion(bf16[140,64,256]{2,1,0:T(8,128)(2,1)} %get-tuple-element.209, s32[1024]{0:T(1024)S(1)} %pad_clamp_fusion.4), kind=kCustom, calls=%fused_computation.clone.1 | custom fusion | bytes 4194560 | tf_op jit(solution)/shard_map/while/body/eval_jaxpr/jit(_take)/gather | solution.py:113
  188.1 2.9 bitcast_select_fusion.3
  192.5 1.0 constant_dynamic-slice_fusion.4
  193.5 2.6 fusion.52
  197.7 0.8 fusion.54
  198.5 0.9 copy_dynamic-update-slice_fusion.4
  202.7 4.4 %gather_fusion = bf16[64,64,256]{2,1,0:T(8,128)(2,1)} fusion(bf16[140,64,256]{2,1,0:T(8,128)(2,1)} %get-tuple-element.209, s32[1024]{0:T(1024)S(1)} %pad_clamp_fusion.4), kind=kCustom, calls=%fused_computation.clone.1 | custom fusion | bytes 4194560 | tf_op jit(solution)/shard_map/while/body/eval_jaxpr/jit(_take)/gather | solution.py:113
  207.2 2.9 bitcast_select_fusion.3
  211.6 1.0 constant_dynamic-slice_fusion.4
  212.6 2.6 fusion.52
  216.8 0.8 fusion.54
  217.5 0.9 copy_dynamic-update-slice_fusion.4
  221.8 4.4 %gather_fusion = bf16[64,64,256]{2,1,0:T(8,128)(2,1)} fusion(bf16[140,64,256]{2,1,0:T(8,128)(2,1)} %get-tuple-element.209, s32[1024]{0:T(1024)S(1)} %pad_clamp_fusion.4), kind=kCustom, calls=%fused_computation.clone.1 | custom fusion | bytes 4194560 | tf_op jit(solution)/shard_map/while/body/eval_jaxpr/jit(_take)/gather | solution.py:113
  226.3 2.9 bitcast_select_fusion.3
  230.6 1.0 constant_dynamic-slice_fusion.4
  231.7 2.6 fusion.52
  235.9 0.8 fusion.54
  236.6 0.9 copy_dynamic-update-slice_fusion.4
  240.9 4.4 %gather_fusion = bf16[64,64,256]{2,1,0:T(8,128)(2,1)} fusion(bf16[140,64,256]{2,1,0:T(8,128)(2,1)} %get-tuple-element.209, s32[1024]{0:T(1024)S(1)} %pad_clamp_fusion.4), kind=kCustom, calls=%fused_computation.clone.1 | custom fusion | bytes 4194560 | tf_op jit(solution)/shard_map/while/body/eval_jaxpr/jit(_take)/gather | solution.py:113
  245.4 2.9 bitcast_select_fusion.3
  249.7 1.0 constant_dynamic-slice_fusion.4
  250.8 2.6 fusion.52
  254.9 0.8 fusion.54
  255.7 0.9 copy_dynamic-update-slice_fusion.4
  256.6 1.8 copy.41
  258.4 7.0 %convolution_convert_fusion = bf16[768,2048]{1,0:T(8,128)(2,1)} fusion(bf16[768,1024]{1,0:T(8,128)(2,1)S(1)} %bitcast.84, bf16[1024,2048]{1,0:T(8,128)(2,1)} %param.12), kind=kOutput, calls=%fused_computation.35 | convolution fusion | flops 3222798336 | bytes 8912896 | tf_op jit(solution)/shard_map/dot_general | solution.py:124
  265.4 4.8 %all-to-all-start.2 = ((bf16[4,192,2048]{2,1,0:T(8,128)(2,1)}), bf16[4,192,2048]{2,1,0:T(8,128)(2,1)}, u32[]{:S(2)}, u32[]{:S(2)}) async-start(bf16[4,192,2048]{2,1,0:T(8,128)(2,1)} %bitcast.83), calls=%async_computation.2 | async-start | bytes 6291456 | tf_op jit(solution)/shard_map/all_to_all | solution.py:22
  270.9 37.3 %all-to-all-done.2 = bf16[4,192,2048]{2,1,0:T(8,128)(2,1)} async-done(((bf16[4,192,2048]{2,1,0:T(8,128)(2,1)}), bf16[4,192,2048]{2,1,0:T(8,128)(2,1)}, u32[]{:S(2)}, u32[]{:S(2)}) %all-to-all-start.2) | async-done | bytes 3145760 | tf_op jit(solution)/shard_map/all_to_all | solution.py:22
  308.2 3.6 %reduce_sum.41 = bf16[192,2048]{1,0:T(8,128)(2,1)} reduce(bf16[4,192,2048]{2,1,0:T(8,128)(2,1)} %all-to-all-done.2, bf16[]{:T(256)} %constant.68.clone.1), dimensions={0}, to_apply=%region_9.10 | reduce | flops 1179648 | bytes 3932162 | tf_op jit(solution)/shard_map/reduce_sum | solution.py:23
  (162 shorter events, 26.1 us)
Async XLA Ops:
  0.6 14.3 %copy-start = (bf16[768,2048]{1,0:T(8,128)(2,1)S(1)}, bf16[768,2048]{1,0:T(8,128)(2,1)}, u32[]{:S(2)}) copy-start(bf16[768,2048]{1,0:T(8,128)(2,1)} %param.8) | copy-start | bytes 9437188
  2.2 15.0 %copy-start.2 = (s32[64,12]{1,0:T(8,128)}, s32[64,12]{1,0:T(8,128)S(1)}, u32[]{:S(2)}) copy-start(s32[64,12]{1,0:T(8,128)S(1)} %broadcast_add_fusion.1) | copy-start | bytes 9220
  3.2 18.6 %all-to-all-start = ((s32[64,1,2]{2,1,0:T(1,128)}), s32[64,1,2]{2,1,0:T(1,128)}, u32[]{:S(2)}, u32[]{:S(2)}) async-start(s32[64,1,2]{2,1,0:T(1,128)} %copy.26), calls=%async_computation | async-start | bytes 65536 | tf_op jit(solution)/shard_map/all_to_all | solution.py:89
  14.9 2.3 copy-start.5
  33.9 9.2 %copy-start.3 = (s32[12,32]{1,0:T(8,128)S(1)}, s32[12,32]{1,0:T(8,128)}, u32[]{:S(2)}) copy-start(s32[12,32]{1,0:T(8,128)} %param.13) | copy-start | bytes 4612
  33.9 103.6 %all-to-all-start.1 = ((bf16[64,2,64,256]{3,2,1,0:T(8,128)(2,1)}), bf16[64,2,64,256]{3,2,1,0:T(8,128)(2,1)}, u32[]{:S(2)}, u32[]{:S(2)}) async-start(bf16[64,2,64,256]{3,2,1,0:T(8,128)(2,1)} %broadcast_select_fusion), calls=%async_computation.1 | async-start | bytes 8388608 | tf_op jit(solution)/shard_map/all_to_all | solution.py:92
  157.9 1.6 copy-start.1
  177.0 1.6 copy-start.1
  196.1 1.6 copy-start.1
  215.2 1.6 copy-start.1
  234.3 1.6 copy-start.1
  253.3 1.6 copy-start.1
  265.4 4.8 %copy-start.4 = (f32[6,2,64,4]{2,1,0,3:T(2,128)S(1)}, f32[6,2,64,4]{2,1,0,3:T(2,128)}, u32[]{:S(2)}) copy-start(f32[6,2,64,4]{2,1,0,3:T(2,128)} %get-tuple-element.51) | copy-start | bytes 36868
  265.4 42.8 %all-to-all-start.2 = ((bf16[4,192,2048]{2,1,0:T(8,128)(2,1)}), bf16[4,192,2048]{2,1,0:T(8,128)(2,1)}, u32[]{:S(2)}, u32[]{:S(2)}) async-start(bf16[4,192,2048]{2,1,0:T(8,128)(2,1)} %bitcast.83), calls=%async_computation.2 | async-start | bytes 6291456 | tf_op jit(solution)/shard_map/all_to_all | solution.py:22
where the time goes:
time: 314 us; the launch traced here: 312 us
  waiting for transfers between devices  119 us (38%)
  local copies, waits for them, and re-layouts  68.1 us (22%)
  other arithmetic  47.2 us (15%)
  matrix products  35.9 us (11%)
  starting transfers between devices  24.8 us (8%)
  loops' own time  15.4 us (5%)
    all_to_all x1, waiting for transfers between devices, local(): lax.all_to_all(reply_blocks, 'kv', split_axis=0, concat_axis=0, tiled=True)  77.8 us
    all_to_all x1, waiting for transfers between devices, summed_on_arrival(): lax.all_to_all(split_up(value, dim, devices), axis, 0, 0, tiled=True)  37.3 us
    gather x6, local copies, waits for them, and re-layouts, one_group(): jnp.take(key_table, located, axis=0)  26.1 us
    select_n x6, other arithmetic, one_group(): jnp.take(key_table, located, axis=0)  17.5 us
    another operation x1, loops' own time, local(): heads_out, log_total = lax.map(one_group, group_starts)  15.4 us
    dot_general x6, matrix products, attend(): jnp.einsum('gqhr,gkr->ghqk', query_part, key_rows, preferred_element_type...  15.4 us
    all_to_all x1, starting transfers between devices, local(): lax.all_to_all(request, 'kv', split_axis=0, concat_axis=0, tiled=True)  11.7 us
    dynamic_update_slice x12, local copies, waits for them, and re-layouts, local(): heads_out, log_total = lax.map(one_group, group_starts)  9.13 us
  transfers between devices with their start and end apart: 3, of which 3 were waited for; matrix products, arithmetic and copies ran while one was open for 7% of the time, Pallas kernels for 0%

commit v1 on v0

v1 whole, which is shorter than its diff:
```python
import functools

import jax
import jax.numpy as jnp
from jax import lax
from jax.experimental import pallas as pl
from jax.experimental.pallas import tpu as pltpu
from jax.sharding import PartitionSpec as P

EPS = 1e-06
KV = 64
TP = 4
GRP = 8
BLK = 64
HALF = 32
R = 256
PER = 12
NSEL = 32
OWN = TP * KV
SLOTS = OWN + 2 * PER
ROWS = PER * BLK
HEADS = 4


def remote(src, dst, send_sem, recv_sem, kv, tp):
    return pltpu.make_async_remote_copy(
        src_ref=src,
        dst_ref=dst,
        send_sem=send_sem,
        recv_sem=recv_sem,
        device_id={"kv": kv, "tp": tp},
        device_id_type=pl.DeviceIdType.MESH,
    )


def fetch_kernel(
    tok_hbm, wl_ref, gain_ref, wq_hbm, req_ref,
    table_ref, q_ref,
    tok_v, wq_v, own_v, sendbuf, reqin, req_smem,
    tok_sem, wq_sem, loc_sem, rs_sem, rr_sem, ds_sem, dr_sem, xs_sem, xl_sem, xr_sem, xd_sem,
):
    me = lax.axis_index("kv")
    x = lax.axis_index("tp")
    mz = me // GRP
    myc = me % GRP
    left = (x + TP - 1) % TP
    right = (x + 1) % TP

    reqin[...] = jnp.zeros_like(reqin)
    barrier = pltpu.get_barrier_semaphore()

    @pl.loop(0, KV)
    def _(i):
        @pl.when(i != me)
        def _():
            pl.semaphore_signal(
                barrier, inc=1, device_id={"kv": i, "tp": x}, device_id_type=pl.DeviceIdType.MESH
            )

    for nb in (left, right):
        pl.semaphore_signal(
            barrier, inc=1, device_id={"kv": me, "tp": nb}, device_id_type=pl.DeviceIdType.MESH
        )

    def tok_copy(i):
        rows = pl.ds(i * 128, 128)
        return pltpu.make_async_copy(tok_hbm.at[rows], tok_v.at[rows], tok_sem.at[i])

    def wq_copy(h):
        cols = pl.ds(h * R, R)
        return pltpu.make_async_copy(wq_hbm.at[:, cols], wq_v.at[:, cols], wq_sem.at[h])

    for i in range(6):
        tok_copy(i).start()
    for h in range(HEADS):
        wq_copy(h).start()
    for i in range(6):
        tok_copy(i).wait()
        p = jnp.dot(tok_v[i * 128 : (i + 1) * 128, :], wl_ref[...], preferred_element_type=jnp.float32)
        inv = lax.rsqrt(jnp.mean(p * p, axis=-1, keepdims=True) + EPS)
        lat = (p * inv * gain_ref[...]).astype(jnp.bfloat16)
        own_v[4 * i : 4 * i + 4] = lat.reshape(4, HALF, R)
        table_ref[OWN + 4 * i : OWN + 4 * i + 4] = lat.reshape(4, HALF, R)

    pl.semaphore_wait(barrier, KV - 1 + 2)

    def req_copy(i):
        return remote(req_ref.at[i], reqin.at[me], rs_sem.at[i], rr_sem.at[me], i, x)

    @pl.loop(0, me)
    def _(i):
        req_copy(i).start()

    @pl.loop(me + 1, KV)
    def _(i):
        remote(req_ref.at[i], reqin.at[i], rs_sem.at[i], rr_sem.at[i], i, x).wait_recv()

    to_smem = pltpu.make_async_copy(reqin, req_smem, loc_sem)
    to_smem.start()
    to_smem.wait()

    def data_copy(d):
        return remote(
            sendbuf.at[d],
            table_ref.at[x * KV + me],
            ds_sem.at[d],
            dr_sem.at[jnp.where(d // GRP == mz, GRP + myc, mz)],
            d,
            x,
        )

    @pl.loop(0, GRP - mz)
    def _(s):
        base = (GRP - 1 - s) * GRP

        @pl.loop(0, GRP)
        def _(k):
            d = base + (myc + k) % GRP

            @pl.when(d > me)
            def _():
                sendbuf[d] = own_v[req_smem[d, 0, 0]]

        @pl.loop(0, GRP)
        def _(k):
            d = base + (myc + k) % GRP

            @pl.when(d > me)
            def _():
                data_copy(d).start()

    for h in range(HEADS):
        wq_copy(h).wait()
        q = jnp.dot(tok_v[...], wq_v[:, h * R : (h + 1) * R], preferred_element_type=jnp.float32)
        q_ref[:, h * R : (h + 1) * R] = (q.astype(jnp.bfloat16).astype(jnp.float32) * (R ** -0.5)).astype(jnp.bfloat16)

    def region(quarter, z):
        return table_ref.at[pl.ds(quarter * KV + z * GRP, GRP)]

    def to_right(z):
        return remote(region(x, z), region(x, z), xs_sem.at[0, z], xl_sem.at[z], me, right)

    def to_left(z):
        return remote(region(x, z), region(x, z), xs_sem.at[1, z], xr_sem.at[z], me, left)

    def pass_right(z):
        return remote(region(left, z), region(left, z), xs_sem.at[2, z], xd_sem.at[z], me, right)

    def pass_left(z):
        return remote(region(right, z), region(right, z), xs_sem.at[2, z], xd_sem.at[z], me, left)

    def group_done(z):
        pltpu.make_async_copy(region(x, z), region(x, z), dr_sem.at[z]).wait()

    for dist in (1, 7, 2, 6, 3, 5, 4):
        @pl.when(mz >= dist)
        def _(dist=dist):
            z = mz - dist
            group_done(z)
            to_right(z).start()
            to_left(z).start()

    @pl.when(myc > 0)
    def _():
        @pl.loop(0, myc)
        def _(k):
            one = table_ref.at[x * KV + mz * GRP + k]
            pltpu.make_async_copy(one, one, dr_sem.at[GRP + k]).wait()

        to_right(mz).start()
        to_left(mz).start()

    for dist in (1, 7, 2, 6, 3, 5, 4, 0):
        z = mz - dist

        @pl.when((z >= 0) & ((dist != 0) | (myc > 0)))
        def _(z=z):
            to_right(z).wait_recv()
            to_left(z).wait_recv()

            @pl.when(z % 2 == 0)
            def _():
                pass_right(z).start()

            @pl.when(z % 2 == 1)
            def _():
                pass_left(z).start()

    for dist in (1, 7, 2, 6, 3, 5, 4, 0):
        z = mz - dist

        @pl.when((z >= 0) & ((dist != 0) | (myc > 0)))
        def _(z=z):
            pass_right(z).wait_recv()
            to_right(z).wait_send()
            to_left(z).wait_send()
            pass_right(z).wait_send()

    @pl.loop(0, me)
    def _(i):
        req_copy(i).wait_send()

    @pl.loop(me + 1, KV)
    def _(d):
        data_copy(d).wait_send()


def fetch(tokens, w_latent, gain, w_query, req):
    vmem = pl.BlockSpec(memory_space=pltpu.VMEM)
    anyspace = pl.BlockSpec(memory_space=pl.ANY)
    dma = pltpu.SemaphoreType.DMA
    return pl.pallas_call(
        fetch_kernel,
        out_shape=(
            jax.ShapeDtypeStruct((SLOTS, HALF, R), jnp.bfloat16),
            jax.ShapeDtypeStruct((ROWS, HEADS * R), jnp.bfloat16),
        ),
        in_specs=[anyspace, vmem, vmem, anyspace, vmem],
        out_specs=(vmem, vmem),
        scratch_shapes=[
            pltpu.VMEM(tokens.shape, jnp.bfloat16),
            pltpu.VMEM(w_query.shape, jnp.bfloat16),
            pltpu.VMEM((2 * PER, HALF, R), jnp.bfloat16),
            pltpu.VMEM((KV, HALF, R), jnp.bfloat16),
            pltpu.VMEM((KV, 1, 128), jnp.int32),
            pltpu.SMEM((KV, 1, 128), jnp.int32),
            dma((6,)),
            dma((HEADS,)),
            dma,
            dma((KV,)),
            dma((KV,)),
            dma((KV,)),
            dma((2 * GRP,)),
            dma((3, GRP)),
            dma((GRP,)),
            dma((GRP,)),
            dma((GRP,)),
        ],
        compiler_params=pltpu.CompilerParams(
            collective_id=0, has_side_effects=True, vmem_limit_bytes=48 * 1024 * 1024
        ),
        name="fetch",
    )(tokens, w_latent, gain, w_query, req)


def attend_kernel(idx_ref, cnt_ref, q_ref, table_ref, out_ref, log_ref, kbuf, s_scr, p_scr):
    g = pl.program_id(0)
    base = g * (2 * NSEL)
    for j in range(2 * NSEL):
        kbuf[j * HALF : (j + 1) * HALF, :] = table_ref[idx_ref[base + j]]
    q = jnp.concatenate([q_ref[:, h * R : (h + 1) * R] for h in range(HEADS)], axis=0)
    live = cnt_ref[g] * BLK
    rows = HEADS * BLK
    step = 512
    top = None
    for c in range(NSEL * BLK // step):
        s = lax.dot_general(
            q, kbuf[c * step : (c + 1) * step, :], (((1,), (1,)), ((), ())),
            preferred_element_type=jnp.float32,
        )
        col = lax.broadcasted_iota(jnp.int32, (rows, step), 1)
        ok = col + c * step < live
        if c == 0:
            t = lax.broadcasted_iota(jnp.int32, (rows, step), 0) % BLK
            ok = ok & ((col >= BLK) | (col <= t))
        s = jnp.where(ok, s, -jnp.inf)
        s_scr[:, c * step : (c + 1) * step] = s
        for k in range(step // 128):
            part = s[:, k * 128 : (k + 1) * 128]
            top = part if top is None else jnp.maximum(top, part)
    peak = jnp.max(top, axis=1, keepdims=True)
    total = None
    for c in range(NSEL * BLK // step):
        e = jnp.exp(s_scr[:, c * step : (c + 1) * step] - peak)
        p_scr[:, c * step : (c + 1) * step] = e.astype(jnp.bfloat16)
        for k in range(step // 128):
            part = e[:, k * 128 : (k + 1) * 128]
            total = part if total is None else total + part
    mass = jnp.sum(total, axis=1, keepdims=True)
    o = jnp.dot(p_scr[...], kbuf[...], preferred_element_type=jnp.float32) / mass
    logs = peak + jnp.log(mass)
    for h in range(HEADS):
        out_ref[:, h * R : (h + 1) * R] = o[h * BLK : (h + 1) * BLK].astype(jnp.bfloat16)
        log_ref[:, h : h + 1] = logs[h * BLK : (h + 1) * BLK]


def attention(idx, cnt, q, table):
    return pl.pallas_call(
        attend_kernel,
        grid_spec=pltpu.PrefetchScalarGridSpec(
            num_scalar_prefetch=2,
            grid=(PER,),
            in_specs=[
                pl.BlockSpec((BLK, HEADS * R), lambda g, *_: (g, 0)),
                pl.BlockSpec((SLOTS, HALF, R), lambda g, *_: (0, 0, 0)),
            ],
            out_specs=[
                pl.BlockSpec((BLK, HEADS * R), lambda g, *_: (g, 0)),
                pl.BlockSpec((BLK, HEADS), lambda g, *_: (g, 0)),
            ],
            scratch_shapes=[
                pltpu.VMEM((NSEL * BLK, R), jnp.bfloat16),
                pltpu.VMEM((HEADS * BLK, NSEL * BLK), jnp.float32),
                pltpu.VMEM((HEADS * BLK, NSEL * BLK), jnp.bfloat16),
            ],
        ),
        out_shape=(
            jax.ShapeDtypeStruct((ROWS, HEADS * R), jnp.bfloat16),
            jax.ShapeDtypeStruct((ROWS, HEADS), jnp.float32),
        ),
        compiler_params=pltpu.CompilerParams(vmem_limit_bytes=48 * 1024 * 1024),
        name="attend",
    )(idx, cnt, q, table)


def plan(chosen):
    me = lax.axis_index("kv")
    x = lax.axis_index("tp")
    flat = chosen.reshape(PER * NSEL)
    valid = flat >= 0
    owner = jnp.where(valid, flat // PER, -1)
    owners = jnp.arange(KV, dtype=jnp.int32)
    hit = owner[None, :] == owners[:, None]
    lo = jnp.min(jnp.where(hit, flat[None, :], KV * PER), axis=1)
    hi = jnp.max(jnp.where(hit, flat[None, :], -1), axis=1)
    pick = jnp.where(x < 2, lo, hi) - owners * PER
    req = jnp.clip(pick, 0, PER - 1) * 2 + x % 2
    req = jnp.broadcast_to(req[:, None, None], (KV, 1, 128))
    later = jnp.any(hit & (flat[None, :] > lo[:, None]), axis=0)
    own0 = OWN + 2 * (flat - me * PER)
    far0 = 2 * KV * later.astype(jnp.int32) + owner
    mine = owner == me
    first = jnp.where(valid, jnp.where(mine, own0, far0), OWN)
    second = jnp.where(valid, first + jnp.where(mine, 1, KV), OWN)
    idx = jnp.stack([first, second], axis=1).reshape(-1)
    cnt = jnp.sum((chosen >= 0).astype(jnp.int32), axis=1)
    return req, idx, cnt


def local(tokens, w_query, w_latent, latent_gain, w_output, chosen):
    req, idx, cnt = plan(chosen)
    table, q = fetch(tokens, w_latent, latent_gain.reshape(1, R), w_query, req)
    heads, logs = attention(idx, cnt, q, table)
    partial = jnp.dot(heads, w_output, preferred_element_type=jnp.float32).astype(jnp.bfloat16)
    parts = lax.all_to_all(partial.reshape(TP, ROWS // TP, -1), "tp", 0, 0, tiled=True)
    attended = jnp.sum(parts.astype(jnp.float32), axis=0).astype(jnp.bfloat16)
    return attended, logs


def solution(mesh):
    placed = (P("kv", None), P(None, "tp"), P(), P(), P("tp", None), P("kv", None))
    return jax.shard_map(
        local,
        mesh=mesh,
        in_specs=placed,
        out_specs=(P(("kv", "tp"), None), P("kv", "tp")),
        check_vma=False,
    )
```

time: 314 us -> 150 us (0.48)
  the two profiles are of different devices: /device:TPU:48 before, /device:TPU:248 now
where the time goes in v1:
time: 150 us
  Pallas kernels  94.2 us (63%)
  waiting for transfers between devices  36.8 us (25%)
  local copies, waits for them, and re-layouts  6.06 us (4%)
  matrix products  4.81 us (3%)
  starting transfers between devices  3.7 us (2%)
  other arithmetic  3.51 us (2%)
    pallas_call x1, Pallas kernels, fetch(): pl.pallas_call(fetch_kernel, out_shape=(jax.ShapeDtypeStruct((SLOTS, HALF...  71.5 us
    all_to_all x1, waiting for transfers between devices, local(): lax.all_to_all(partial.reshape(TP, ROWS // TP, -1), 'tp', 0, 0, tiled=True)  36.8 us
    pallas_call x1, Pallas kernels, attention(): pl.pallas_call(attend_kernel, grid_spec=pltpu.PrefetchScalarGridSpec(num_...  22.7 us
    dot_general x1, matrix products, local(): jnp.dot(heads, w_output, preferred_element_type=jnp.float32)  4.81 us
    unnamed x9, local copies, waits for them, and re-layouts  4.55 us
    all_to_all x1, starting transfers between devices, local(): lax.all_to_all(partial.reshape(TP, ROWS // TP, -1), 'tp', 0, 0, tiled=True)  3.7 us
  transfers between devices with their start and end apart: 1, of which 1 were waited for; matrix products, arithmetic and copies ran while one was open for 1% of the time, Pallas kernels for 0%

profile of v1, /device:TPU:248, one launch (start us, length us, event | category | flops | bytes accessed | tf_op | source)
XLA Modules:
  0.0 149.8 jit_solution(15450983148131547763)
XLA Ops:
  0.6 0.8 reshape.195
  1.4 0.7 fusion.2
  2.1 0.1 select_reduce_fusion
  2.3 0.1 fusion.1
  2.4 0.1 and.35
  2.5 0.8 multiply_add_fusion
  3.3 0.1 add.78
  3.4 0.1 div.27
  3.5 0.1 ge.32
  3.6 0.1 copy.19
  3.7 0.1 reshape.196.idx_ref
  3.9 0.1 broadcast_in_dim.38.req_ref
  4.0 0.0 copy-start
  4.0 1.9 %copy-done = bf16[768,2048]{1,0:T(8,128)(2,1)S(1)} copy-done((bf16[768,2048]{1,0:T(8,128)(2,1)S(1)}, bf16[768,2048]{1,0:T(8,128)(2,1)}, u32[]{:S(2)}) %copy-start) | copy-done | bytes 3145752
  5.9 0.0 copy-start.1
  5.9 1.2 copy-done.1
  7.2 0.0 copy-start.2
  7.2 0.7 copy-done.2
  7.8 71.5 %fetch.1 = (bf16[280,32,256]{2,1,0:T(8,128)(2,1)}, bf16[768,1024]{1,0:T(8,128)(2,1)S(1)}) custom-call(bf16[768,2048]{1,0:T(8,128)(2,1)S(1)} %copy-done, bf16[2048,256]{1,0:T(8,128)(2,1)S(1)} %copy-done.1, f32[1,256]{1,0:T(1,128)S(1)} %bitcast.4, bf16[2048,1024]{1,0:T(8,128)(2,1)} %wq_hbm.1, s32[64,1,128]{2,1,0:T(1,128)S(1)} %broadcast_in_dim.38.req_ref), custom_call_target="tpu_custom_call" | custom-call | tf_op jit(solution)/shard_map/fetch/pallas_call | solution.py:212
  79.3 0.0 copy-start.3
  79.3 22.7 %attend.1 = (bf16[768,1024]{1,0:T(8,128)(2,1)S(1)}, f32[768,4]{1,0:T(8,128)S(1)}) custom-call(s32[768]{0:T(1024)S(1)} %reshape.196.idx_ref, s32[12]{0:T(128)S(1)} %get-tuple-element.26.cnt_ref, bf16[768,1024]{1,0:T(8,128)(2,1)S(1)} %get-tuple-element.6.q_ref, bf16[280,32,256]{2,1,0:T(8,128)(2,1)} %get-tuple-element.7.table_ref), custom_call_target="tpu_custom_call" | custom-call | tf_op jit(solution)/shard_map/attend/pallas_call | solution.py:288
  102.0 0.0 copy-done.3
  102.0 4.8 %convolution_convert_fusion = bf16[768,2048]{1,0:T(8,128)(2,1)} fusion(bf16[768,1024]{1,0:T(8,128)(2,1)S(1)} %get-tuple-element.8, bf16[1024,2048]{1,0:T(8,128)(2,1)S(1)} %copy-done.3), kind=kOutput, calls=%fused_computation | convolution fusion | flops 3222798336 | bytes 8912896 | tf_op jit(solution)/shard_map/dot_general | solution.py:344
  106.8 3.7 %all-to-all-start = ((bf16[4,192,2048]{2,1,0:T(8,128)(2,1)}), bf16[4,192,2048]{2,1,0:T(8,128)(2,1)S(1)}, u32[]{:S(2)}, u32[]{:S(2)}) async-start(bf16[4,192,2048]{2,1,0:T(8,128)(2,1)} %bitcast.5), calls=%async_computation | async-start | bytes 6291456 | tf_op jit(solution)/shard_map/all_to_all | solution.py:345
  110.5 0.8 copy.20
  111.3 36.8 %all-to-all-done = bf16[4,192,2048]{2,1,0:T(8,128)(2,1)S(1)} async-done(((bf16[4,192,2048]{2,1,0:T(8,128)(2,1)}), bf16[4,192,2048]{2,1,0:T(8,128)(2,1)S(1)}, u32[]{:S(2)}, u32[]{:S(2)}) %all-to-all-start) | async-done | bytes 3145760 | tf_op jit(solution)/shard_map/all_to_all | solution.py:345
  148.1 1.7 %reduce_sum.22 = bf16[192,2048]{1,0:T(8,128)(2,1)} reduce(bf16[4,192,2048]{2,1,0:T(8,128)(2,1)S(1)} %all-to-all-done, bf16[]{:T(256)} %constant.59.clone.1), dimensions={0}, to_apply=%region_4.5 | reduce | flops 1179648 | bytes 3932162 | tf_op jit(solution)/shard_map/reduce_sum | solution.py:346
  (5 shorter events, 0.1 us)
Async XLA Ops:
  4.0 1.9 %copy-start = (bf16[768,2048]{1,0:T(8,128)(2,1)S(1)}, bf16[768,2048]{1,0:T(8,128)(2,1)}, u32[]{:S(2)}) copy-start(bf16[768,2048]{1,0:T(8,128)(2,1)} %tok_hbm.1) | copy-start | bytes 9437188
  5.9 1.2 copy-start.1
  7.2 0.7 copy-start.2
  79.3 22.7 %copy-start.3 = (bf16[1024,2048]{1,0:T(8,128)(2,1)S(1)}, bf16[1024,2048]{1,0:T(8,128)(2,1)}, u32[]{:S(2)}) copy-start(bf16[1024,2048]{1,0:T(8,128)(2,1)} %param.10) | copy-start | bytes 12582916
  106.8 41.3 %all-to-all-start = ((bf16[4,192,2048]{2,1,0:T(8,128)(2,1)}), bf16[4,192,2048]{2,1,0:T(8,128)(2,1)S(1)}, u32[]{:S(2)}, u32[]{:S(2)}) async-start(bf16[4,192,2048]{2,1,0:T(8,128)(2,1)} %bitcast.5), calls=%async_computation | async-start | bytes 6291456 | tf_op jit(solution)/shard_map/all_to_all | solution.py:345

commit v2 on v1

--- a/solution.py
+++ b/solution.py
@@ -207,7 +207,7 @@
 
 def fetch(tokens, w_latent, gain, w_query, req):
     vmem = pl.BlockSpec(memory_space=pltpu.VMEM)
-    anyspace = pl.BlockSpec(memory_space=pl.ANY)
+    anyspace = pl.BlockSpec(memory_space=pltpu.HBM)
     dma = pltpu.SemaphoreType.DMA
     return pl.pallas_call(
         fetch_kernel,
@@ -243,74 +243,160 @@
     )(tokens, w_latent, gain, w_query, req)
 
 
-def attend_kernel(idx_ref, cnt_ref, q_ref, table_ref, out_ref, log_ref, kbuf, s_scr, p_scr):
-    g = pl.program_id(0)
-    base = g * (2 * NSEL)
-    for j in range(2 * NSEL):
-        kbuf[j * HALF : (j + 1) * HALF, :] = table_ref[idx_ref[base + j]]
-    q = jnp.concatenate([q_ref[:, h * R : (h + 1) * R] for h in range(HEADS)], axis=0)
-    live = cnt_ref[g] * BLK
+def finish_kernel(
+    idx_ref, cnt_ref, q_ref, table_ref, wo_ref,
+    out_ref, log_ref,
+    kbuf, s_scr, m_scr, heads, stage, got,
+    snd_sem, got_sem,
+):
+    me = lax.axis_index("kv")
+    x = lax.axis_index("tp")
+    left = (x + TP - 1) % TP
+    right = (x + 1) % TP
+    barrier = pltpu.get_barrier_semaphore()
+    for nb in (left, right):
+        pl.semaphore_signal(
+            barrier, inc=1, device_id={"kv": me, "tp": nb}, device_id_type=pl.DeviceIdType.MESH
+        )
+
+    def dest(it):
+        off = jnp.where(it == 0, 2, jnp.where(it == 1, 1, jnp.where(it == 2, 3, 0)))
+        return (x + off) % TP
+
     rows = HEADS * BLK
+    keys = NSEL * BLK
     step = 512
-    top = None
-    for c in range(NSEL * BLK // step):
-        s = lax.dot_general(
-            q, kbuf[c * step : (c + 1) * step, :], (((1,), (1,)), ((), ())),
-            preferred_element_type=jnp.float32,
-        )
-        col = lax.broadcasted_iota(jnp.int32, (rows, step), 1)
-        ok = col + c * step < live
-        if c == 0:
-            t = lax.broadcasted_iota(jnp.int32, (rows, step), 0) % BLK
-            ok = ok & ((col >= BLK) | (col <= t))
-        s = jnp.where(ok, s, -jnp.inf)
-        s_scr[:, c * step : (c + 1) * step] = s
-        for k in range(step // 128):
-            part = s[:, k * 128 : (k + 1) * 128]
-            top = part if top is None else jnp.maximum(top, part)
-    peak = jnp.max(top, axis=1, keepdims=True)
-    total = None
-    for c in range(NSEL * BLK // step):
-        e = jnp.exp(s_scr[:, c * step : (c + 1) * step] - peak)
-        p_scr[:, c * step : (c + 1) * step] = e.astype(jnp.bfloat16)
-        for k in range(step // 128):
-            part = e[:, k * 128 : (k + 1) * 128]
-            total = part if total is None else total + part
-    mass = jnp.sum(total, axis=1, keepdims=True)
-    o = jnp.dot(p_scr[...], kbuf[...], preferred_element_type=jnp.float32) / mass
-    logs = peak + jnp.log(mass)
-    for h in range(HEADS):
-        out_ref[:, h * R : (h + 1) * R] = o[h * BLK : (h + 1) * BLK].astype(jnp.bfloat16)
-        log_ref[:, h : h + 1] = logs[h * BLK : (h + 1) * BLK]
-
-
-def attention(idx, cnt, q, table):
+
+    def scores(b, slot):
+        for j in range(2 * NSEL):
+            kbuf[slot, j * HALF : (j + 1) * HALF, :] = table_ref[idx_ref[b * (2 * NSEL) + j]]
+        here = pl.ds(pl.multiple_of(b * BLK, BLK), BLK)
+        q = jnp.concatenate([q_ref[here, h * R : (h + 1) * R] for h in range(HEADS)], axis=0)
+        live = cnt_ref[b] * BLK
+        top = None
+        for c in range(keys // step):
+            s = lax.dot_general(
+                q, kbuf[slot, c * step : (c + 1) * step, :], (((1,), (1,)), ((), ())),
+                preferred_element_type=jnp.float32,
+            )
+            col = lax.broadcasted_iota(jnp.int32, (rows, step), 1)
+            ok = col + c * step < live
+            if c == 0:
+                t = lax.broadcasted_iota(jnp.int32, (rows, step), 0) % BLK
+                ok = ok & ((col >= BLK) | (col <= t))
+            s = jnp.where(ok, s, -jnp.inf)
+            s_scr[slot, :, c * step : (c + 1) * step] = s
+            for k in range(step // 128):
+                part = s[:, k * 128 : (k + 1) * 128]
+                top = part if top is None else jnp.maximum(top, part)
+        m_scr[slot] = top
+
+    def values(b, slot, j):
+        peak = jnp.max(m_scr[slot], axis=1, keepdims=True)
+        total = None
+        o = None
+        for c in range(keys // step):
+            e = jnp.exp(s_scr[slot, :, c * step : (c + 1) * step] - peak)
+            for k in range(step // 128):
+                part = e[:, k * 128 : (k + 1) * 128]
+                total = part if total is None else total + part
+            oc = jnp.dot(
+                e.astype(jnp.bfloat16), kbuf[slot, c * step : (c + 1) * step, :],
+                preferred_element_type=jnp.float32,
+            )
+            o = oc if o is None else o + oc
+        mass = jnp.sum(total, axis=1, keepdims=True)
+        o = o / mass
+        logs = peak + jnp.log(mass)
+        here = pl.ds(pl.multiple_of(b * BLK, BLK), BLK)
+        for h in range(HEADS):
+            heads[j * BLK : (j + 1) * BLK, h * R : (h + 1) * R] = o[h * BLK : (h + 1) * BLK].astype(jnp.bfloat16)
+            log_ref[here, h : h + 1] = logs[h * BLK : (h + 1) * BLK]
+
+    def move(k):
+        src, slot, nb = (
+            (stage.at[0, 0], 0, right),
+            (stage.at[0, 1], 1, left),
+            (stage.at[1, 1], 2, right),
+            (stage.at[2, 0], 3, left),
+            (stage.at[1, 0], 4, right),
+            (stage.at[2, 1], 5, left),
+        )[k]
+        return remote(src, got.at[slot], snd_sem.at[k], got_sem.at[slot], me, nb)
+
+    scores(3 * dest(0), 0)
+
+    @pl.loop(0, TP)
+    def _(it):
+        b0 = 3 * dest(it)
+        nxt = jnp.where(it == TP - 1, b0, 3 * dest(it + 1))
+        for j in range(3):
+            scores(b0 + j + 1 if j < 2 else nxt, (j + 1) % 3)
+            values(b0 + j, j, j)
+        for n in range(8):
+            part = jnp.dot(heads[...], wo_ref[:, n * 256 : (n + 1) * 256], preferred_element_type=jnp.float32)
+            stage[it, n // 4, :, (n % 4) * 256 : (n % 4 + 1) * 256] = part.astype(jnp.bfloat16)
+
+        @pl.when(it == 0)
+        def _():
+            pl.semaphore_wait(barrier, 2)
+            move(0).start()
+            move(1).start()
+
+        @pl.when(it == 1)
+        def _():
+            move(2).start()
+
+        @pl.when(it == 2)
+        def _():
+            move(3).start()
+
+    f32 = jnp.float32
+    move(0).wait_recv()
+    stage[1, 0] = (stage[1, 0].astype(f32) + got[0].astype(f32)).astype(jnp.bfloat16)
+    move(4).start()
+    move(1).wait_recv()
+    stage[2, 1] = (stage[2, 1].astype(f32) + got[1].astype(f32)).astype(jnp.bfloat16)
+    move(5).start()
+    half = 1024
+    for k, h in ((0, 0), (1, 1)):
+        move(3 - k).wait_recv()
+        move(4 + k).wait_recv()
+        lo = 3 if h == 0 else 2
+        hi = 4 if h == 0 else 5
+        total = stage[3, h].astype(f32) + got[lo].astype(f32) + got[hi].astype(f32)
+        out_ref[:, h * half : (h + 1) * half] = total.astype(jnp.bfloat16)
+    for k in range(6):
+        move(k).wait_send()
+
+
+def finish(idx, cnt, q, table, w_output):
+    vmem = pl.BlockSpec(memory_space=pltpu.VMEM)
+    smem = pl.BlockSpec(memory_space=pltpu.SMEM)
+    part = ROWS // TP
     return pl.pallas_call(
-        attend_kernel,
-        grid_spec=pltpu.PrefetchScalarGridSpec(
-            num_scalar_prefetch=2,
-            grid=(PER,),
-            in_specs=[
-                pl.BlockSpec((BLK, HEADS * R), lambda g, *_: (g, 0)),
-                pl.BlockSpec((SLOTS, HALF, R), lambda g, *_: (0, 0, 0)),
-            ],
-            out_specs=[
-                pl.BlockSpec((BLK, HEADS * R), lambda g, *_: (g, 0)),
-                pl.BlockSpec((BLK, HEADS), lambda g, *_: (g, 0)),
-            ],
-            scratch_shapes=[
-                pltpu.VMEM((NSEL * BLK, R), jnp.bfloat16),
-                pltpu.VMEM((HEADS * BLK, NSEL * BLK), jnp.float32),
-                pltpu.VMEM((HEADS * BLK, NSEL * BLK), jnp.bfloat16),
-            ],
-        ),
+        finish_kernel,
         out_shape=(
-            jax.ShapeDtypeStruct((ROWS, HEADS * R), jnp.bfloat16),
+            jax.ShapeDtypeStruct((part, 2048), jnp.bfloat16),
             jax.ShapeDtypeStruct((ROWS, HEADS), jnp.float32),
         ),
-        compiler_params=pltpu.CompilerParams(vmem_limit_bytes=48 * 1024 * 1024),
-        name="attend",
-    )(idx, cnt, q, table)
+        in_specs=[smem, smem, vmem, vmem, vmem],
+        out_specs=(vmem, vmem),
+        scratch_shapes=[
+            pltpu.VMEM((3, NSEL * BLK, R), jnp.bfloat16),
+            pltpu.VMEM((3, HEADS * BLK, NSEL * BLK), jnp.float32),
+            pltpu.VMEM((3, HEADS * BLK, 128), jnp.float32),
+            pltpu.VMEM((part, HEADS * R), jnp.bfloat16),
+            pltpu.VMEM((TP, 2, part, 1024), jnp.bfloat16),
+            pltpu.VMEM((6, part, 1024), jnp.bfloat16),
+            pltpu.SemaphoreType.DMA((6,)),
+            pltpu.SemaphoreType.DMA((6,)),
+        ],
+        compiler_params=pltpu.CompilerParams(
+            collective_id=1, has_side_effects=True, vmem_limit_bytes=48 * 1024 * 1024
+        ),
+        name="finish",
+    )(idx, cnt, q, table, w_output)
 
 
 def plan(chosen):
@@ -340,10 +426,7 @@
 def local(tokens, w_query, w_latent, latent_gain, w_output, chosen):
     req, idx, cnt = plan(chosen)
     table, q = fetch(tokens, w_latent, latent_gain.reshape(1, R), w_query, req)
-    heads, logs = attention(idx, cnt, q, table)
-    partial = jnp.dot(heads, w_output, preferred_element_type=jnp.float32).astype(jnp.bfloat16)
-    parts = lax.all_to_all(partial.reshape(TP, ROWS // TP, -1), "tp", 0, 0, tiled=True)
-    attended = jnp.sum(parts.astype(jnp.float32), axis=0).astype(jnp.bfloat16)
+    attended, logs = finish(idx, cnt, q, table, w_output)
     return attended, logs
 
 

time: 150 us -> 116 us (0.77)
  waiting for transfers between devices: 36.8 us -> 0 us
  Pallas kernels: 94.2 us -> 107 us
  matrix products: 4.81 us -> 0 us
  starting transfers between devices: 3.7 us -> 0 us
  other arithmetic: 3.51 us -> 1.82 us
    all_to_all x1 -> x0, waiting for transfers between devices: 36.8 us -> none  [local(): lax.all_to_all(partial.reshape(TP, ROWS // TP, -1), 'tp', 0, 0, tiled=True)]
    pallas_call x1, Pallas kernels: 22.7 us -> 35.1 us  [finish(): pl.pallas_call(finish_kernel, out_shape=(jax.ShapeDtypeStruct((part, 2048...]
    dot_general x1 -> x0, matrix products: 4.81 us -> none  [local(): jnp.dot(heads, w_output, preferred_element_type=jnp.float32)]
    all_to_all x1 -> x0, starting transfers between devices: 3.7 us -> none  [local(): lax.all_to_all(partial.reshape(TP, ROWS // TP, -1), 'tp', 0, 0, tiled=True)]
    reduce_sum x1 -> x0, other arithmetic: 1.69 us -> none  [local(): attended = jnp.sum(parts.astype(jnp.float32), axis=0).astype(jnp.bfloat16)]
    unnamed x9 -> x7, local copies, waits for them, and re-layouts: 4.55 us -> 4.67 us
  transfers between devices with their start and end apart: 1 -> 0, of which waited for: 1 -> 0; matrix products, arithmetic and copies ran while one was open for 1% -> 0% of each run, Pallas kernels for 0% -> 0%
where the time goes in v2:
time: 116 us
  Pallas kernels  107 us (92%)
  local copies, waits for them, and re-layouts  6.93 us (6%)
  other arithmetic  1.82 us (2%)
    pallas_call x1, Pallas kernels, fetch(): pl.pallas_call(fetch_kernel, out_shape=(jax.ShapeDtypeStruct((SLOTS, HALF...  71.5 us
    pallas_call x1, Pallas kernels, finish(): pl.pallas_call(finish_kernel, out_shape=(jax.ShapeDtypeStruct((part, 2048...  35.1 us
    unnamed x7, local copies, waits for them, and re-layouts  4.67 us

profile of v2, /device:TPU:248, one launch (start us, length us, event | category | flops | bytes accessed | tf_op | source)
XLA Modules:
  0.0 116.0 jit_solution(16330224114180806654)
XLA Ops:
  0.6 0.8 reshape.192
  1.4 0.1 select_reduce_fusion
  1.6 0.1 fusion.1
  1.7 0.7 fusion.2
  2.4 0.1 and.35
  2.5 0.8 multiply_add_fusion
  3.3 0.1 add.78
  3.4 0.1 div.27
  3.5 0.1 ge.32
  3.6 0.1 broadcast_in_dim.38.req_ref
  3.7 0.1 copy.19
  3.9 0.1 reshape.193.idx_ref
  4.0 0.0 copy-start
  4.0 1.9 %copy-done = bf16[768,2048]{1,0:T(8,128)(2,1)S(1)} copy-done((bf16[768,2048]{1,0:T(8,128)(2,1)S(1)}, bf16[768,2048]{1,0:T(8,128)(2,1)}, u32[]{:S(2)}) %copy-start) | copy-done | bytes 3145752
  5.9 0.0 copy-start.1
  5.9 1.2 %copy-done.1 = bf16[2048,256]{1,0:T(8,128)(2,1)S(1)} copy-done((bf16[2048,256]{1,0:T(8,128)(2,1)S(1)}, bf16[2048,256]{1,0:T(8,128)(2,1)}, u32[]{:S(2)}) %copy-start.1) | copy-done | bytes 1048600
  7.1 0.0 copy-start.2
  7.1 0.7 copy-done.2
  7.8 71.5 %fetch.1 = (bf16[280,32,256]{2,1,0:T(8,128)(2,1)}, bf16[768,1024]{1,0:T(8,128)(2,1)S(1)}) custom-call(bf16[768,2048]{1,0:T(8,128)(2,1)S(1)} %copy-done, bf16[2048,256]{1,0:T(8,128)(2,1)S(1)} %copy-done.1, f32[1,256]{1,0:T(1,128)S(1)} %bitcast.1, bf16[2048,1024]{1,0:T(8,128)(2,1)} %wq_hbm.1, s32[64,1,128]{2,1,0:T(1,128)S(1)} %broadcast_in_dim.38.req_ref), custom_call_target="tpu_custom_call" | custom-call | tf_op jit(solution)/shard_map/fetch/pallas_call | solution.py:212
  79.3 35.1 %finish.1 = (bf16[192,2048]{1,0:T(8,128)(2,1)S(1)}, f32[768,4]{1,0:T(8,128)S(1)}) custom-call(s32[768]{0:T(1024)S(1)} %reshape.193.idx_ref, s32[12]{0:T(128)S(1)} %get-tuple-element.22.cnt_ref, bf16[768,1024]{1,0:T(8,128)(2,1)S(1)} %get-tuple-element.4.q_ref, bf16[280,32,256]{2,1,0:T(8,128)(2,1)} %get-tuple-element.5.table_ref, bf16[1024,2048]{1,0:T(8,128)(2,1)} %wo_ref.1), custom_call_target="tpu_custom_call" | custom-call | tf_op jit(solution)/shard_map/finish/pallas_call | solution.py:377
  114.4 0.8 copy.20
  115.2 0.9 copy.22
  (5 shorter events, 0.1 us)
Async XLA Ops:
  4.0 1.9 %copy-start = (bf16[768,2048]{1,0:T(8,128)(2,1)S(1)}, bf16[768,2048]{1,0:T(8,128)(2,1)}, u32[]{:S(2)}) copy-start(bf16[768,2048]{1,0:T(8,128)(2,1)} %tok_hbm.1) | copy-start | bytes 9437188
  5.9 1.2 %copy-start.1 = (bf16[2048,256]{1,0:T(8,128)(2,1)S(1)}, bf16[2048,256]{1,0:T(8,128)(2,1)}, u32[]{:S(2)}) copy-start(bf16[2048,256]{1,0:T(8,128)(2,1)} %wl_ref.1) | copy-start | bytes 3145732
  7.1 0.7 copy-start.2

commit v3 on v2

v3 whole, which is shorter than its diff:
```python
import functools

import jax
import jax.numpy as jnp
from jax import lax
from jax.experimental import pallas as pl
from jax.experimental.pallas import tpu as pltpu
from jax.sharding import PartitionSpec as P

EPS = 1e-06
KV = 64
TP = 4
GRP = 8
BLK = 64
HALF = 32
R = 256
PER = 12
NSEL = 32
OWN = TP * KV
SLOTS = OWN + 2 * PER
ROWS = PER * BLK
HEADS = 4


def remote(src, dst, send_sem, recv_sem, kv, tp):
    return pltpu.make_async_remote_copy(
        src_ref=src,
        dst_ref=dst,
        send_sem=send_sem,
        recv_sem=recv_sem,
        device_id={"kv": kv, "tp": tp},
        device_id_type=pl.DeviceIdType.MESH,
    )


def kernel(
    tok_hbm, wq_hbm, wl_hbm, gain_ref, wo_hbm, chosen_ref,
    out_ref, log_ref,
    tok_v, wq_v, wl_v, wo_v, own_v, sendbuf, table_ref, q_ref,
    req_v, reqin, idx_v, req_smem, idx_ref,
    kbuf, s_scr, m_scr, heads, stage, got,
    tok_sem, wq_sem, wl_sem, wo_sem, loc_sem, rs_sem, rr_sem, ds_sem, dr_sem,
    xs_sem, xl_sem, xr_sem, xd_sem, snd_sem, got_sem,
):
    me = lax.axis_index("kv")
    x = lax.axis_index("tp")
    mz = me // GRP
    myc = me % GRP
    left = (x + TP - 1) % TP
    right = (x + 1) % TP
    reqin[...] = jnp.zeros_like(reqin)
    barrier = pltpu.get_barrier_semaphore()

    @pl.loop(0, KV)
    def _(i):
        @pl.when(i != me)
        def _():
            pl.semaphore_signal(
                barrier, inc=1, device_id={"kv": i, "tp": x}, device_id_type=pl.DeviceIdType.MESH
            )

    for nb in (left, right):
        pl.semaphore_signal(
            barrier, inc=1, device_id={"kv": me, "tp": nb}, device_id_type=pl.DeviceIdType.MESH
        )

    def tok_copy(i):
        rows = pl.ds(i * 128, 128)
        return pltpu.make_async_copy(tok_hbm.at[rows], tok_v.at[rows], tok_sem.at[i])

    def wq_copy(h):
        cols = pl.ds(h * R, R)
        return pltpu.make_async_copy(wq_hbm.at[:, cols], wq_v.at[:, cols], wq_sem.at[h])

    wl_copy = pltpu.make_async_copy(wl_hbm, wl_v, wl_sem)
    wo_copy = pltpu.make_async_copy(wo_hbm, wo_v, wo_sem)
    wl_copy.start()
    for i in range(6):
        tok_copy(i).start()

    def hits(shape, g):
        c = jnp.broadcast_to(chosen_ref[g : g + 1, :].reshape((1,) * (len(shape) - 1) + (NSEL,)), shape)
        return c, ((c * 683) >> 13) == lax.broadcasted_iota(jnp.int32, shape, 0)

    far = jnp.full((KV, 1, NSEL), KV * PER, jnp.int32)
    near = jnp.full((KV, 1, NSEL), -1, jnp.int32)
    for g in range(PER):
        c, hit = hits((KV, 1, NSEL), g)
        far = jnp.minimum(far, jnp.where(hit, c, KV * PER))
        near = jnp.maximum(near, jnp.where(hit, c, -1))
    lo = jnp.min(far, axis=2, keepdims=True)
    hi = jnp.max(near, axis=2, keepdims=True)
    own0 = lax.broadcasted_iota(jnp.int32, (KV, 1, 1), 0) * PER
    pick = jnp.clip(jnp.where(x < 2, lo, hi) - own0, 0, PER - 1) * 2 + x % 2
    req_v[...] = jnp.broadcast_to(pick, req_v.shape)

    pl.semaphore_wait(barrier, KV - 1 + 2)

    def req_copy(i):
        return remote(req_v.at[i], reqin.at[me], rs_sem.at[i], rr_sem.at[me], i, x)

    @pl.loop(0, me)
    def _(i):
        req_copy(i).start()

    wl_copy.wait()
    for i in range(6):
        tok_copy(i).wait()
        p = jnp.dot(tok_v[i * 128 : (i + 1) * 128, :], wl_v[...], preferred_element_type=jnp.float32)
        inv = lax.rsqrt(jnp.mean(p * p, axis=-1, keepdims=True) + EPS)
        lat = (p * inv * gain_ref[...]).astype(jnp.bfloat16)
        own_v[4 * i : 4 * i + 4] = lat.reshape(4, HALF, R)
        table_ref[OWN + 4 * i : OWN + 4 * i + 4] = lat.reshape(4, HALF, R)

    for h in range(HEADS):
        wq_copy(h).start()
    wo_copy.start()

    @pl.loop(me + 1, KV)
    def _(i):
        remote(req_v.at[i], reqin.at[i], rs_sem.at[i], rr_sem.at[i], i, x).wait_recv()

    to_smem = pltpu.make_async_copy(reqin, req_smem, loc_sem)
    to_smem.start()
    to_smem.wait()

    def data_copy(d):
        return remote(
            sendbuf.at[d],
            table_ref.at[x * KV + me],
            ds_sem.at[d],
            dr_sem.at[jnp.where(d // GRP == mz, GRP + myc, mz)],
            d,
            x,
        )

    def each(delta, action):
        @pl.when(mz + delta < GRP)
        def _():
            @pl.loop(0, GRP)
            def _(k):
                d = (mz + delta) * GRP + (myc + k) % GRP

                @pl.when(d > me)
                def _():
                    action(d)

    def fill(d):
        sendbuf[d] = own_v[req_smem[d, 0, 0]]

    order = (7, 6, 4, 5, 3, 2, 1, 0)
    for s, delta in enumerate(order):
        each(delta, fill)
        if s >= 2:
            each(order[s - 2], lambda d: data_copy(d).wait_send())
        each(delta, lambda d: data_copy(d).start())

    far = jnp.full((KV, NSEL), KV * PER, jnp.int32)
    for g in range(PER):
        c, hit = hits((KV, NSEL), g)
        far = jnp.minimum(far, jnp.where(hit, c, KV * PER))
    lo = jnp.min(far, axis=1, keepdims=True)
    for g in range(PER):
        c, hit = hits((KV, NSEL), g)
        later = jnp.max(jnp.where(hit & (c > lo), 1, 0), axis=0, keepdims=True)
        c = chosen_ref[g : g + 1, :]
        owner = (c * 683) >> 13
        mine = owner == me
        valid = c >= 0
        first = jnp.where(mine, OWN + 2 * (c - me * PER), 2 * KV * later + owner)
        second = first + jnp.where(mine, 1, KV)
        idx_v[0, g : g + 1, 0:NSEL] = jnp.where(valid, first, OWN)
        idx_v[1, g : g + 1, 0:NSEL] = jnp.where(valid, second, OWN)
        live = jnp.sum(jnp.where(valid, 1, 0), axis=1, keepdims=True)
        idx_v[2, g : g + 1, :] = jnp.broadcast_to(live, (1, 128))
    idx_copy = pltpu.make_async_copy(idx_v, idx_ref, loc_sem)
    idx_copy.start()

    def region(quarter, z):
        return table_ref.at[pl.ds(quarter * KV + z * GRP, GRP)]

    def to_right(z):
        return remote(region(x, z), region(x, z), xs_sem.at[0, z], xl_sem.at[z], me, right)

    def to_left(z):
        return remote(region(x, z), region(x, z), xs_sem.at[1, z], xr_sem.at[z], me, left)

    def pass_right(z):
        return remote(region(left, z), region(left, z), xs_sem.at[2, z], xd_sem.at[z], me, right)

    def pass_left(z):
        return remote(region(right, z), region(right, z), xs_sem.at[2, z], xd_sem.at[z], me, left)

    near_first = (1, 2, 7, 3, 6, 5, 4)
    for dist in near_first:
        @pl.when(mz >= dist)
        def _(dist=dist):
            z = mz - dist
            pltpu.make_async_copy(region(x, z), region(x, z), dr_sem.at[z]).wait()
            to_right(z).start()
            to_left(z).start()

    @pl.when(myc > 0)
    def _():
        @pl.loop(0, myc)
        def _(k):
            one = table_ref.at[x * KV + mz * GRP + k]
            pltpu.make_async_copy(one, one, dr_sem.at[GRP + k]).wait()

        to_right(mz).start()
        to_left(mz).start()

    for h in range(HEADS):
        wq_copy(h).wait()
        q = jnp.dot(tok_v[...], wq_v[:, h * R : (h + 1) * R], preferred_element_type=jnp.float32)
        q_ref[:, h * R : (h + 1) * R] = (q.astype(jnp.bfloat16).astype(jnp.float32) * (R ** -0.5)).astype(jnp.bfloat16)

    for dist in near_first + (0,):
        z = mz - dist

        @pl.when((z >= 0) & ((dist != 0) | (myc > 0)))
        def _(z=z):
            to_right(z).wait_recv()
            to_left(z).wait_recv()

            @pl.when(z % 2 == 0)
            def _():
                pass_right(z).start()

            @pl.when(z % 2 == 1)
            def _():
                pass_left(z).start()

    idx_copy.wait()
    wo_copy.wait()
    for dist in near_first + (0,):
        z = mz - dist

        @pl.when((z >= 0) & ((dist != 0) | (myc > 0)))
        def _(z=z):
            pass_right(z).wait_recv()

    def dest(it):
        off = jnp.where(it == 0, 2, jnp.where(it == 1, 1, jnp.where(it == 2, 3, 0)))
        return (x + off) % TP

    rows = HEADS * BLK
    keys = NSEL * BLK
    step = 512

    def scores(b, slot):
        for j in range(2 * NSEL):
            kbuf[slot, j * HALF : (j + 1) * HALF, :] = table_ref[idx_ref[j % 2, b, j // 2]]
        here = pl.ds(pl.multiple_of(b * BLK, BLK), BLK)
        q = jnp.concatenate([q_ref[here, h * R : (h + 1) * R] for h in range(HEADS)], axis=0)
        live = idx_ref[2, b, 0] * BLK
        top = None
        for c in range(keys // step):
            s = lax.dot_general(
                q, kbuf[slot, c * step : (c + 1) * step, :], (((1,), (1,)), ((), ())),
                preferred_element_type=jnp.float32,
            )
            col = lax.broadcasted_iota(jnp.int32, (rows, step), 1)
            ok = col + c * step < live
            if c == 0:
                t = lax.broadcasted_iota(jnp.int32, (rows, step), 0) % BLK
                ok = ok & ((col >= BLK) | (col <= t))
            s = jnp.where(ok, s, -jnp.inf)
            s_scr[slot, :, c * step : (c + 1) * step] = s
            for k in range(step // 128):
                part = s[:, k * 128 : (k + 1) * 128]
                top = part if top is None else jnp.maximum(top, part)
        m_scr[slot] = top

    def values(b, slot, j):
        peak = jnp.max(m_scr[slot], axis=1, keepdims=True)
        total = None
        o = None
        for c in range(keys // step):
            e = jnp.exp(s_scr[slot, :, c * step : (c + 1) * step] - peak)
            for k in range(step // 128):
                part = e[:, k * 128 : (k + 1) * 128]
                total = part if total is None else total + part
            oc = jnp.dot(
                e.astype(jnp.bfloat16), kbuf[slot, c * step : (c + 1) * step, :],
                preferred_element_type=jnp.float32,
            )
            o = oc if o is None else o + oc
        mass = jnp.sum(total, axis=1, keepdims=True)
        o = o / mass
        logs = peak + jnp.log(mass)
        here = pl.ds(pl.multiple_of(b * BLK, BLK), BLK)
        for h in range(HEADS):
            heads[j * BLK : (j + 1) * BLK, h * R : (h + 1) * R] = o[h * BLK : (h + 1) * BLK].astype(jnp.bfloat16)
            log_ref[here, h : h + 1] = logs[h * BLK : (h + 1) * BLK]

    def move(k):
        src, slot, nb = (
            (stage.at[0, 0], 0, right),
            (stage.at[0, 1], 1, left),
            (stage.at[1, 1], 2, right),
            (stage.at[2, 0], 3, left),
            (stage.at[1, 0], 4, right),
            (stage.at[2, 1], 5, left),
        )[k]
        return remote(src, got.at[slot], snd_sem.at[k], got_sem.at[slot], me, nb)

    scores(3 * dest(0), 0)

    @pl.loop(0, TP)
    def _(it):
        b0 = 3 * dest(it)
        nxt = jnp.where(it == TP - 1, b0, 3 * dest(it + 1))
        for j in range(3):
            scores(b0 + j + 1 if j < 2 else nxt, (j + 1) % 3)
            values(b0 + j, j, j)
        for n in range(8):
            part = jnp.dot(heads[...], wo_v[:, n * 256 : (n + 1) * 256], preferred_element_type=jnp.float32)
            stage[it, n // 4, :, (n % 4) * 256 : (n % 4 + 1) * 256] = part.astype(jnp.bfloat16)

        @pl.when(it == 0)
        def _():
            move(0).start()
            move(1).start()

        @pl.when(it == 1)
        def _():
            move(2).start()

        @pl.when(it == 2)
        def _():
            move(3).start()

    f32 = jnp.float32
    move(0).wait_recv()
    stage[1, 0] = (stage[1, 0].astype(f32) + got[0].astype(f32)).astype(jnp.bfloat16)
    move(4).start()
    move(1).wait_recv()
    stage[2, 1] = (stage[2, 1].astype(f32) + got[1].astype(f32)).astype(jnp.bfloat16)
    move(5).start()
    half = 1024
    for k, h in ((0, 0), (1, 1)):
        move(3 - k).wait_recv()
        move(4 + k).wait_recv()
        lo = 3 if h == 0 else 2
        hi = 4 if h == 0 else 5
        total = stage[3, h].astype(f32) + got[lo].astype(f32) + got[hi].astype(f32)
        out_ref[:, h * half : (h + 1) * half] = total.astype(jnp.bfloat16)
    for k in range(6):
        move(k).wait_send()

    for dist in near_first + (0,):
        z = mz - dist

        @pl.when((z >= 0) & ((dist != 0) | (myc > 0)))
        def _(z=z):
            to_right(z).wait_send()
            to_left(z).wait_send()
            pass_right(z).wait_send()

    for delta in order[-2:]:
        each(delta, lambda d: data_copy(d).wait_send())

    @pl.loop(0, me)
    def _(i):
        req_copy(i).wait_send()


def local(tokens, w_query, w_latent, latent_gain, w_output, chosen):
    vmem = pl.BlockSpec(memory_space=pltpu.VMEM)
    hbm = pl.BlockSpec(memory_space=pltpu.HBM)
    dma = pltpu.SemaphoreType.DMA
    bf16 = jnp.bfloat16
    part = ROWS // TP
    return pl.pallas_call(
        kernel,
        out_shape=(
            jax.ShapeDtypeStruct((part, 2048), bf16),
            jax.ShapeDtypeStruct((ROWS, HEADS), jnp.float32),
        ),
        in_specs=[hbm, hbm, hbm, vmem, hbm, vmem],
        out_specs=(vmem, vmem),
        scratch_shapes=[
            pltpu.VMEM(tokens.shape, bf16),
            pltpu.VMEM(w_query.shape, bf16),
            pltpu.VMEM(w_latent.shape, bf16),
            pltpu.VMEM(w_output.shape, bf16),
            pltpu.VMEM((2 * PER, HALF, R), bf16),
            pltpu.VMEM((KV, HALF, R), bf16),
            pltpu.VMEM((SLOTS, HALF, R), bf16),
            pltpu.VMEM((ROWS, HEADS * R), bf16),
            pltpu.VMEM((KV, 1, 128), jnp.int32),
            pltpu.VMEM((KV, 1, 128), jnp.int32),
            pltpu.VMEM((3, 16, 128), jnp.int32),
            pltpu.SMEM((KV, 1, 128), jnp.int32),
            pltpu.SMEM((3, 16, 128), jnp.int32),
            pltpu.VMEM((3, NSEL * BLK, R), bf16),
            pltpu.VMEM((3, HEADS * BLK, NSEL * BLK), jnp.float32),
            pltpu.VMEM((3, HEADS * BLK, 128), jnp.float32),
            pltpu.VMEM((part, HEADS * R), bf16),
            pltpu.VMEM((TP, 2, part, 1024), bf16),
            pltpu.VMEM((6, part, 1024), bf16),
            dma((6,)),
            dma((HEADS,)),
            dma,
            dma,
            dma,
            dma((KV,)),
            dma((KV,)),
            dma((KV,)),
            dma((2 * GRP,)),
            dma((3, GRP)),
            dma((GRP,)),
            dma((GRP,)),
            dma((GRP,)),
            dma((6,)),
            dma((6,)),
        ],
        compiler_params=pltpu.CompilerParams(
            collective_id=0, has_side_effects=True, vmem_limit_bytes=60 * 1024 * 1024
        ),
        name="layer",
    )(tokens, w_query, w_latent, latent_gain.reshape(1, R), w_output, chosen)


def solution(mesh):
    placed = (P("kv", None), P(None, "tp"), P(), P(), P("tp", None), P("kv", None))
    return jax.shard_map(
        local,
        mesh=mesh,
        in_specs=placed,
        out_specs=(P(("kv", "tp"), None), P("kv", "tp")),
        check_vma=False,
    )
```

time: 116 us -> 105 us (0.905); the launches traced: 116 us -> 103 us
  Pallas kernels: 107 us -> 99 us
  local copies, waits for them, and re-layouts: 6.93 us -> 3.83 us
  other arithmetic: 1.82 us -> 0 us
    pallas_call x2 -> x1, Pallas kernels: 107 us -> 99 us  [local(): pl.pallas_call(kernel, out_shape=(jax.ShapeDtypeStruct((part, 2048), bf16...]
    unnamed x7 -> x1, local copies, waits for them, and re-layouts: 4.67 us -> 2.09 us
where the time goes in v3:
time: 105 us; the launch traced here: 103 us
  Pallas kernels  99 us (94%)
  local copies, waits for them, and re-layouts  3.83 us (4%)
    pallas_call x1, Pallas kernels, local(): pl.pallas_call(kernel, out_shape=(jax.ShapeDtypeStruct((part, 2048), bf16...  99 us

profile of v3, /device:TPU:248, one launch (start us, length us, event | category | flops | bytes accessed | tf_op | source)
XLA Modules:
  0.0 103.5 jit_solution(18105231738077850108)
XLA Ops:
  0.6 99.0 %layer.1 = (bf16[192,2048]{1,0:T(8,128)(2,1)}, f32[768,4]{1,0:T(8,128)}) custom-call(bf16[768,2048]{1,0:T(8,128)(2,1)} %tok_hbm.1, bf16[2048,1024]{1,0:T(8,128)(2,1)} %wq_hbm.1, bf16[2048,256]{1,0:T(8,128)(2,1)} %wl_hbm.1, f32[1,256]{1,0:T(1,128)} %bitcast.1, bf16[1024,2048]{1,0:T(8,128)(2,1)} %wo_hbm.1, s32[12,32]{1,0:T(8,128)} %chosen_ref.1), custom_call_target="tpu_custom_call" | custom-call | tf_op jit(solution)/shard_map/layer/pallas_call | solution.py:375
  99.6 1.7 %copy.8 = f32[768,4]{0,1:T(4,128)} copy(f32[768,4]{1,0:T(8,128)} %get-tuple-element.3) | data formatting | bytes 24576 | tf_op jit(solution)/shard_map/layer/pallas_call | solution.py:375
  101.4 2.1 %copy.10 = bf16[192,2048]{1,0:T(8,128)(2,1)} copy(bf16[192,2048]{1,0:T(8,128)(2,1)} %get-tuple-element.6) | data formatting | bytes 1572864

commit v4 on v3

--- a/solution.py
+++ b/solution.py
@@ -38,7 +38,7 @@
     out_ref, log_ref,
     tok_v, wq_v, wl_v, wo_v, own_v, sendbuf, table_ref, q_ref,
     req_v, reqin, idx_v, req_smem, idx_ref,
-    kbuf, s_scr, m_scr, heads, stage, got,
+    kbuf, s_scr, m_scr, heads, stage, got, log_v,
     tok_sem, wq_sem, wl_sem, wo_sem, loc_sem, rs_sem, rr_sem, ds_sem, dr_sem,
     xs_sem, xl_sem, xr_sem, xd_sem, snd_sem, got_sem,
 ):
@@ -148,13 +148,53 @@
     def fill(d):
         sendbuf[d] = own_v[req_smem[d, 0, 0]]
 
-    order = (7, 6, 4, 5, 3, 2, 1, 0)
-    for s, delta in enumerate(order):
-        each(delta, fill)
-        if s >= 2:
+    order = (0, 1, 7, 2, 6, 3, 5, 4)
+
+    def send_group(s):
+        each(order[s], fill)
+        if s >= 3:
             each(order[s - 2], lambda d: data_copy(d).wait_send())
-        each(delta, lambda d: data_copy(d).start())
-
+        each(order[s], lambda d: data_copy(d).start())
+
+    def project_query(h):
+        wq_copy(h).wait()
+        q = jnp.dot(tok_v[...], wq_v[:, h * R : (h + 1) * R], preferred_element_type=jnp.float32)
+        q_ref[:, h * R : (h + 1) * R] = (q.astype(jnp.bfloat16).astype(jnp.float32) * (R ** -0.5)).astype(jnp.bfloat16)
+
+    def region(quarter, z):
+        return table_ref.at[pl.ds(quarter * KV + z * GRP, GRP)]
+
+    def to_right(z):
+        return remote(region(x, z), region(x, z), xs_sem.at[0, z], xl_sem.at[z], me, right)
+
+    def to_left(z):
+        return remote(region(x, z), region(x, z), xs_sem.at[1, z], xr_sem.at[z], me, left)
+
+    def pass_right(z):
+        return remote(region(left, z), region(left, z), xs_sem.at[2, z], xd_sem.at[z], me, right)
+
+    def pass_left(z):
+        return remote(region(right, z), region(right, z), xs_sem.at[2, z], xd_sem.at[z], me, left)
+
+    send_group(0)
+    send_group(1)
+    send_group(2)
+    project_query(0)
+    project_query(1)
+    @pl.when(myc > 0)
+    def _():
+        @pl.loop(0, myc)
+        def _(k):
+            one = table_ref.at[x * KV + mz * GRP + k]
+            pltpu.make_async_copy(one, one, dr_sem.at[GRP + k]).wait()
+
+        to_right(mz).start()
+        to_left(mz).start()
+
+    send_group(3)
+    project_query(2)
+    send_group(4)
+    project_query(3)
     far = jnp.full((KV, NSEL), KV * PER, jnp.int32)
     for g in range(PER):
         c, hit = hits((KV, NSEL), g)
@@ -176,50 +216,23 @@
     idx_copy = pltpu.make_async_copy(idx_v, idx_ref, loc_sem)
     idx_copy.start()
 
-    def region(quarter, z):
-        return table_ref.at[pl.ds(quarter * KV + z * GRP, GRP)]
-
-    def to_right(z):
-        return remote(region(x, z), region(x, z), xs_sem.at[0, z], xl_sem.at[z], me, right)
-
-    def to_left(z):
-        return remote(region(x, z), region(x, z), xs_sem.at[1, z], xr_sem.at[z], me, left)
-
-    def pass_right(z):
-        return remote(region(left, z), region(left, z), xs_sem.at[2, z], xd_sem.at[z], me, right)
-
-    def pass_left(z):
-        return remote(region(right, z), region(right, z), xs_sem.at[2, z], xd_sem.at[z], me, left)
-
-    near_first = (1, 2, 7, 3, 6, 5, 4)
-    for dist in near_first:
+    dists = (0, 1, 7, 2, 6, 3, 5, 4)
+
+    def have(dist):
+        return (mz >= dist) if dist else (myc > 0)
+
+    def share(dist):
         @pl.when(mz >= dist)
-        def _(dist=dist):
+        def _():
             z = mz - dist
             pltpu.make_async_copy(region(x, z), region(x, z), dr_sem.at[z]).wait()
             to_right(z).start()
             to_left(z).start()
 
-    @pl.when(myc > 0)
-    def _():
-        @pl.loop(0, myc)
-        def _(k):
-            one = table_ref.at[x * KV + mz * GRP + k]
-            pltpu.make_async_copy(one, one, dr_sem.at[GRP + k]).wait()
-
-        to_right(mz).start()
-        to_left(mz).start()
-
-    for h in range(HEADS):
-        wq_copy(h).wait()
-        q = jnp.dot(tok_v[...], wq_v[:, h * R : (h + 1) * R], preferred_element_type=jnp.float32)
-        q_ref[:, h * R : (h + 1) * R] = (q.astype(jnp.bfloat16).astype(jnp.float32) * (R ** -0.5)).astype(jnp.bfloat16)
-
-    for dist in near_first + (0,):
-        z = mz - dist
-
-        @pl.when((z >= 0) & ((dist != 0) | (myc > 0)))
-        def _(z=z):
+    def relay(dist):
+        @pl.when(have(dist))
+        def _():
+            z = mz - dist
             to_right(z).wait_recv()
             to_left(z).wait_recv()
 
@@ -231,12 +244,31 @@
             def _():
                 pass_left(z).start()
 
+    share(1)
+    send_group(5)
+    share(7)
+    relay(0)
+    send_group(6)
+    share(2)
+    relay(1)
+    send_group(7)
+    share(6)
+    relay(7)
+    share(3)
+    relay(2)
+    share(5)
+    relay(6)
+    share(4)
+    relay(3)
+    relay(5)
+    relay(4)
+
     idx_copy.wait()
     wo_copy.wait()
-    for dist in near_first + (0,):
+    for dist in dists:
         z = mz - dist
 
-        @pl.when((z >= 0) & ((dist != 0) | (myc > 0)))
+        @pl.when(have(dist))
         def _(z=z):
             pass_right(z).wait_recv()
 
@@ -292,18 +324,25 @@
         here = pl.ds(pl.multiple_of(b * BLK, BLK), BLK)
         for h in range(HEADS):
             heads[j * BLK : (j + 1) * BLK, h * R : (h + 1) * R] = o[h * BLK : (h + 1) * BLK].astype(jnp.bfloat16)
-            log_ref[here, h : h + 1] = logs[h * BLK : (h + 1) * BLK]
+            log_v[here, h : h + 1] = logs[h * BLK : (h + 1) * BLK]
+
+    half = 1024
+    quarter = 256
+
+    def project(it, lo, hi):
+        for n in range(2048 // quarter):
+            part = jnp.dot(
+                heads[lo:hi, :], wo_v[:, n * quarter : (n + 1) * quarter], preferred_element_type=jnp.float32
+            )
+            c = n * quarter % half
+            stage[it, n * quarter // half, lo:hi, c : c + quarter] = part.astype(jnp.bfloat16)
+
+    def first(h):
+        return remote(stage.at[0, h], got.at[h], snd_sem.at[h], got_sem.at[h], me, right if h == 0 else left)
 
     def move(k):
-        src, slot, nb = (
-            (stage.at[0, 0], 0, right),
-            (stage.at[0, 1], 1, left),
-            (stage.at[1, 1], 2, right),
-            (stage.at[2, 0], 3, left),
-            (stage.at[1, 0], 4, right),
-            (stage.at[2, 1], 5, left),
-        )[k]
-        return remote(src, got.at[slot], snd_sem.at[k], got_sem.at[slot], me, nb)
+        it, h, nb = ((1, 1, right), (2, 0, left), (1, 0, right), (2, 1, left))[k]
+        return remote(stage.at[it, h], got.at[2 + k], snd_sem.at[2 + k], got_sem.at[2 + k], me, nb)
 
     scores(3 * dest(0), 0)
 
@@ -314,51 +353,47 @@
         for j in range(3):
             scores(b0 + j + 1 if j < 2 else nxt, (j + 1) % 3)
             values(b0 + j, j, j)
-        for n in range(8):
-            part = jnp.dot(heads[...], wo_v[:, n * 256 : (n + 1) * 256], preferred_element_type=jnp.float32)
-            stage[it, n // 4, :, (n % 4) * 256 : (n % 4 + 1) * 256] = part.astype(jnp.bfloat16)
+        project(it, 0, 3 * BLK)
 
         @pl.when(it == 0)
         def _():
+            first(0).start()
+            first(1).start()
+
+        @pl.when(it == 1)
+        def _():
             move(0).start()
+
+        @pl.when(it == 2)
+        def _():
             move(1).start()
 
-        @pl.when(it == 1)
-        def _():
-            move(2).start()
-
-        @pl.when(it == 2)
-        def _():
-            move(3).start()
-
     f32 = jnp.float32
-    move(0).wait_recv()
-    stage[1, 0] = (stage[1, 0].astype(f32) + got[0].astype(f32)).astype(jnp.bfloat16)
-    move(4).start()
-    move(1).wait_recv()
-    stage[2, 1] = (stage[2, 1].astype(f32) + got[1].astype(f32)).astype(jnp.bfloat16)
-    move(5).start()
-    half = 1024
-    for k, h in ((0, 0), (1, 1)):
-        move(3 - k).wait_recv()
-        move(4 + k).wait_recv()
-        lo = 3 if h == 0 else 2
-        hi = 4 if h == 0 else 5
-        total = stage[3, h].astype(f32) + got[lo].astype(f32) + got[hi].astype(f32)
+    for h in range(2):
+        first(h).wait_recv()
+        stage[1 + h, h] = (stage[1 + h, h].astype(f32) + got[h].astype(f32)).astype(jnp.bfloat16)
+        move(2 + h).start()
+    log_ref[...] = jnp.transpose(log_v[...])[0:HEADS]
+    for h in range(2):
+        move(1 - h).wait_recv()
+        move(2 + h).wait_recv()
+        total = stage[3, h].astype(f32) + got[3 - h].astype(f32) + got[4 + h].astype(f32)
         out_ref[:, h * half : (h + 1) * half] = total.astype(jnp.bfloat16)
-    for k in range(6):
+    for h in range(2):
+        first(h).wait_send()
+    for k in range(4):
         move(k).wait_send()
 
-    for dist in near_first + (0,):
+    for dist in dists:
         z = mz - dist
 
-        @pl.when((z >= 0) & ((dist != 0) | (myc > 0)))
+        @pl.when(have(dist))
         def _(z=z):
             to_right(z).wait_send()
             to_left(z).wait_send()
             pass_right(z).wait_send()
 
-    for delta in order[-2:]:
+    for delta in order[:1] + order[-2:]:
         each(delta, lambda d: data_copy(d).wait_send())
 
     @pl.loop(0, me)
@@ -372,11 +407,11 @@
     dma = pltpu.SemaphoreType.DMA
     bf16 = jnp.bfloat16
     part = ROWS // TP
-    return pl.pallas_call(
+    attended, logs = pl.pallas_call(
         kernel,
         out_shape=(
             jax.ShapeDtypeStruct((part, 2048), bf16),
-            jax.ShapeDtypeStruct((ROWS, HEADS), jnp.float32),
+            jax.ShapeDtypeStruct((HEADS, ROWS), jnp.float32),
         ),
         in_specs=[hbm, hbm, hbm, vmem, hbm, vmem],
         out_specs=(vmem, vmem),
@@ -400,6 +435,7 @@
             pltpu.VMEM((part, HEADS * R), bf16),
             pltpu.VMEM((TP, 2, part, 1024), bf16),
             pltpu.VMEM((6, part, 1024), bf16),
+            pltpu.VMEM((ROWS, 128), jnp.float32),
             dma((6,)),
             dma((HEADS,)),
             dma,
@@ -417,10 +453,11 @@
             dma((6,)),
         ],
         compiler_params=pltpu.CompilerParams(
-            collective_id=0, has_side_effects=True, vmem_limit_bytes=60 * 1024 * 1024
+            collective_id=0, has_side_effects=True, vmem_limit_bytes=53 * 1024 * 1024
         ),
         name="layer",
     )(tokens, w_query, w_latent, latent_gain.reshape(1, R), w_output, chosen)
+    return attended, logs.T
 
 
 def solution(mesh):

time: 105 us -> 101 us (0.962)
  the two profiles are of different devices: /device:TPU:248 before, /device:TPU:192 now
where the time goes in v4:
time: 101 us
  Pallas kernels  97.7 us (97%)
  local copies, waits for them, and re-layouts  2.85 us (3%)
    pallas_call x1, Pallas kernels, local(): pl.pallas_call(kernel, out_shape=(jax.ShapeDtypeStruct((part, 2048), bf16...  97.7 us
    unnamed x6, local copies, waits for them, and re-layouts  2.85 us

profile of v4, /device:TPU:192, one launch (start us, length us, event | category | flops | bytes accessed | tf_op | source)
XLA Modules:
  0.0 101.2 jit_solution(15934892898268652578)
XLA Ops:
  0.6 0.0 copy-start
  0.6 0.7 copy-done
  1.3 0.0 copy-start.1
  1.3 0.7 copy-done.1
  2.0 97.7 %layer.1 = (bf16[192,2048]{1,0:T(8,128)(2,1)S(1)}, f32[4,768]{1,0:T(4,128)S(1)}) custom-call(bf16[768,2048]{1,0:T(8,128)(2,1)} %tok_hbm.1, bf16[2048,1024]{1,0:T(8,128)(2,1)} %wq_hbm.1, bf16[2048,256]{1,0:T(8,128)(2,1)} %wl_hbm.1, f32[1,256]{1,0:T(1,128)S(1)} %bitcast.3, bf16[1024,2048]{1,0:T(8,128)(2,1)} %wo_hbm.1, s32[12,32]{1,0:T(8,128)S(1)} %copy-done), custom_call_target="tpu_custom_call" | custom-call | tf_op jit(solution)/shard_map/layer/pallas_call | solution.py:410
  99.7 0.9 copy.10
  100.6 0.6 copy.11
Async XLA Ops:
  0.6 0.7 copy-start
  1.3 0.7 copy-start.1

commit v5 on v4

--- a/solution.py
+++ b/solution.py
@@ -152,8 +152,8 @@
 
     def send_group(s):
         each(order[s], fill)
-        if s >= 3:
-            each(order[s - 2], lambda d: data_copy(d).wait_send())
+        if s >= 5:
+            each(order[s - 4], lambda d: data_copy(d).wait_send())
         each(order[s], lambda d: data_copy(d).start())
 
     def project_query(h):
@@ -176,11 +176,11 @@
     def pass_left(z):
         return remote(region(right, z), region(right, z), xs_sem.at[2, z], xd_sem.at[z], me, left)
 
-    send_group(0)
-    send_group(1)
-    send_group(2)
+    for s in range(5):
+        send_group(s)
     project_query(0)
     project_query(1)
+
     @pl.when(myc > 0)
     def _():
         @pl.loop(0, myc)
@@ -191,10 +191,11 @@
         to_right(mz).start()
         to_left(mz).start()
 
-    send_group(3)
+    send_group(5)
     project_query(2)
-    send_group(4)
+    send_group(6)
     project_query(3)
+    send_group(7)
     far = jnp.full((KV, NSEL), KV * PER, jnp.int32)
     for g in range(PER):
         c, hit = hits((KV, NSEL), g)
@@ -221,8 +222,8 @@
     def have(dist):
         return (mz >= dist) if dist else (myc > 0)
 
-    def share(dist):
-        @pl.when(mz >= dist)
+    def share(dist, only=None):
+        @pl.when((mz >= dist) if only is None else (mz == only))
         def _():
             z = mz - dist
             pltpu.make_async_copy(region(x, z), region(x, z), dr_sem.at[z]).wait()
@@ -245,21 +246,19 @@
                 pass_left(z).start()
 
     share(1)
-    send_group(5)
     share(7)
     relay(0)
-    send_group(6)
     share(2)
     relay(1)
-    send_group(7)
-    share(6)
     relay(7)
+    share(6, GRP - 1)
     share(3)
     relay(2)
+    share(6, 6)
     share(5)
     relay(6)
+    relay(3)
     share(4)
-    relay(3)
     relay(5)
     relay(4)
 
@@ -393,7 +392,7 @@
             to_left(z).wait_send()
             pass_right(z).wait_send()
 
-    for delta in order[:1] + order[-2:]:
+    for delta in order[:1] + order[-4:]:
         each(delta, lambda d: data_copy(d).wait_send())
 
     @pl.loop(0, me)

time: 101 us -> 93.7 us (0.928)
  the two profiles are of different devices: /device:TPU:192 before, /device:TPU:248 now
where the time goes in v5:
time: 93.7 us; the launch traced here: 92 us
  Pallas kernels  88.5 us (94%)
  local copies, waits for them, and re-layouts  2.85 us (3%)
    pallas_call x1, Pallas kernels, local(): pl.pallas_call(kernel, out_shape=(jax.ShapeDtypeStruct((part, 2048), bf16...  88.5 us
    unnamed x6, local copies, waits for them, and re-layouts  2.85 us

profile of v5, /device:TPU:248, one launch (start us, length us, event | category | flops | bytes accessed | tf_op | source)
XLA Modules:
  0.0 92.0 jit_solution(18443821972281058880)
XLA Ops:
  0.6 0.0 copy-start
  0.6 0.7 copy-done
  1.3 0.0 copy-start.1
  1.3 0.7 copy-done.1
  2.0 88.5 %layer.1 = (bf16[192,2048]{1,0:T(8,128)(2,1)S(1)}, f32[4,768]{1,0:T(4,128)S(1)}) custom-call(bf16[768,2048]{1,0:T(8,128)(2,1)} %tok_hbm.1, bf16[2048,1024]{1,0:T(8,128)(2,1)} %wq_hbm.1, bf16[2048,256]{1,0:T(8,128)(2,1)} %wl_hbm.1, f32[1,256]{1,0:T(1,128)S(1)} %bitcast.3, bf16[1024,2048]{1,0:T(8,128)(2,1)} %wo_hbm.1, s32[12,32]{1,0:T(8,128)S(1)} %copy-done), custom_call_target="tpu_custom_call" | custom-call | tf_op jit(solution)/shard_map/layer/pallas_call | solution.py:409
  90.5 0.9 copy.10
  91.4 0.6 copy.11
Async XLA Ops:
  0.6 0.7 copy-start
  1.3 0.7 copy-start.1

commit v6 on v5

--- a/solution.py
+++ b/solution.py
@@ -37,7 +37,7 @@
     tok_hbm, wq_hbm, wl_hbm, gain_ref, wo_hbm, chosen_ref,
     out_ref, log_ref,
     tok_v, wq_v, wl_v, wo_v, own_v, sendbuf, table_ref, q_ref,
-    req_v, reqin, idx_v, req_smem, idx_ref,
+    req_v, idx_v, reqin, idx_ref,
     kbuf, s_scr, m_scr, heads, stage, got, log_v,
     tok_sem, wq_sem, wl_sem, wo_sem, loc_sem, rs_sem, rr_sem, ds_sem, dr_sem,
     xs_sem, xl_sem, xr_sem, xd_sem, snd_sem, got_sem,
@@ -48,7 +48,6 @@
     myc = me % GRP
     left = (x + TP - 1) % TP
     right = (x + 1) % TP
-    reqin[...] = jnp.zeros_like(reqin)
     barrier = pltpu.get_barrier_semaphore()
 
     @pl.loop(0, KV)
@@ -116,14 +115,6 @@
         wq_copy(h).start()
     wo_copy.start()
 
-    @pl.loop(me + 1, KV)
-    def _(i):
-        remote(req_v.at[i], reqin.at[i], rs_sem.at[i], rr_sem.at[i], i, x).wait_recv()
-
-    to_smem = pltpu.make_async_copy(reqin, req_smem, loc_sem)
-    to_smem.start()
-    to_smem.wait()
-
     def data_copy(d):
         return remote(
             sendbuf.at[d],
@@ -145,12 +136,16 @@
                 def _():
                     action(d)
 
+    def asked(d):
+        remote(req_v.at[d], reqin.at[d], rs_sem.at[d], rr_sem.at[d], d, x).wait_recv()
+
     def fill(d):
-        sendbuf[d] = own_v[req_smem[d, 0, 0]]
+        sendbuf[d] = own_v[reqin[d, 0, 0]]
 
     order = (0, 1, 7, 2, 6, 3, 5, 4)
 
     def send_group(s):
+        each(order[s], asked)
         each(order[s], fill)
         if s >= 5:
             each(order[s - 4], lambda d: data_copy(d).wait_send())
@@ -257,8 +252,8 @@
     share(6, 6)
     share(5)
     relay(6)
+    share(4)
     relay(3)
-    share(4)
     relay(5)
     relay(4)
 
@@ -423,7 +418,6 @@
             pltpu.VMEM((KV, HALF, R), bf16),
             pltpu.VMEM((SLOTS, HALF, R), bf16),
             pltpu.VMEM((ROWS, HEADS * R), bf16),
-            pltpu.VMEM((KV, 1, 128), jnp.int32),
             pltpu.VMEM((KV, 1, 128), jnp.int32),
             pltpu.VMEM((3, 16, 128), jnp.int32),
             pltpu.SMEM((KV, 1, 128), jnp.int32),

time: 93.7 us -> 91.8 us (0.980)
  Pallas kernels: 88.5 us -> 87.1 us
    pallas_call x1, Pallas kernels: 88.5 us -> 87.1 us  [local(): pl.pallas_call(kernel, out_shape=(jax.ShapeDtypeStruct((part, 2048), bf16...]
where the time goes in v6:
time: 91.8 us; the launch traced here: 90.6 us
  Pallas kernels  87.1 us (95%)
  local copies, waits for them, and re-layouts  2.85 us (3%)
    pallas_call x1, Pallas kernels, local(): pl.pallas_call(kernel, out_shape=(jax.ShapeDtypeStruct((part, 2048), bf16...  87.1 us
    unnamed x6, local copies, waits for them, and re-layouts  2.85 us

profile of v6, /device:TPU:248, one launch (start us, length us, event | category | flops | bytes accessed | tf_op | source)
XLA Modules:
  0.0 90.6 jit_solution(3547969114811038483)
XLA Ops:
  0.6 0.0 copy-start
  0.6 0.7 copy-done
  1.3 0.0 copy-start.1
  1.3 0.7 copy-done.1
  2.0 87.1 %layer.1 = (bf16[192,2048]{1,0:T(8,128)(2,1)S(1)}, f32[4,768]{1,0:T(4,128)S(1)}) custom-call(bf16[768,2048]{1,0:T(8,128)(2,1)} %tok_hbm.1, bf16[2048,1024]{1,0:T(8,128)(2,1)} %wq_hbm.1, bf16[2048,256]{1,0:T(8,128)(2,1)} %wl_hbm.1, f32[1,256]{1,0:T(1,128)S(1)} %bitcast.3, bf16[1024,2048]{1,0:T(8,128)(2,1)} %wo_hbm.1, s32[12,32]{1,0:T(8,128)S(1)} %copy-done), custom_call_target="tpu_custom_call" | custom-call | tf_op jit(solution)/shard_map/layer/pallas_call | solution.py:404
  89.2 0.9 copy.10
  90.0 0.6 copy.11
Async XLA Ops:
  0.6 0.7 copy-start
  1.3 0.7 copy-start.1

commit v7 on v6

--- a/solution.py
+++ b/solution.py
@@ -147,8 +147,6 @@
     def send_group(s):
         each(order[s], asked)
         each(order[s], fill)
-        if s >= 5:
-            each(order[s - 4], lambda d: data_copy(d).wait_send())
         each(order[s], lambda d: data_copy(d).start())
 
     def project_query(h):
@@ -387,7 +385,7 @@
             to_left(z).wait_send()
             pass_right(z).wait_send()
 
-    for delta in order[:1] + order[-4:]:
+    for delta in order:
         each(delta, lambda d: data_copy(d).wait_send())
 
     @pl.loop(0, me)

time: 91.8 us -> 92 us (level)
  no operation moved by 1% of the time
where the time goes in v7:
time: 92 us; the launch traced here: 90.7 us
  Pallas kernels  87.2 us (95%)
  local copies, waits for them, and re-layouts  2.85 us (3%)
    pallas_call x1, Pallas kernels, local(): pl.pallas_call(kernel, out_shape=(jax.ShapeDtypeStruct((part, 2048), bf16...  87.2 us
    unnamed x6, local copies, waits for them, and re-layouts  2.85 us

profile of v7, /device:TPU:248, one launch (start us, length us, event | category | flops | bytes accessed | tf_op | source)
XLA Modules:
  0.0 90.7 jit_solution(15630772599781579638)
XLA Ops:
  0.6 0.0 copy-start
  0.6 0.7 copy-done
  1.3 0.0 copy-start.1
  1.3 0.7 copy-done.1
  2.0 87.2 %layer.1 = (bf16[192,2048]{1,0:T(8,128)(2,1)S(1)}, f32[4,768]{1,0:T(4,128)S(1)}) custom-call(bf16[768,2048]{1,0:T(8,128)(2,1)} %tok_hbm.1, bf16[2048,1024]{1,0:T(8,128)(2,1)} %wq_hbm.1, bf16[2048,256]{1,0:T(8,128)(2,1)} %wl_hbm.1, f32[1,256]{1,0:T(1,128)S(1)} %bitcast.3, bf16[1024,2048]{1,0:T(8,128)(2,1)} %wo_hbm.1, s32[12,32]{1,0:T(8,128)S(1)} %copy-done), custom_call_target="tpu_custom_call" | custom-call | tf_op jit(solution)/shard_map/layer/pallas_call | solution.py:402
  89.2 0.9 copy.10
  90.1 0.6 copy.11
Async XLA Ops:
  0.6 0.7 copy-start
  1.3 0.7 copy-start.1
